TPU v7x, 32 devices: a whole 2x2x4 slice. The times are simulated.
32 devices in a mesh: ep: 4 (over y, x), tp: 8 (over z, core).
Axes of the slice: x: 2, y: 2, z: 4, core: 2. Of those that a mesh axis runs over, the one named last changes fastest.
Arguments:
- queries: bfloat16 [4096, 1024], P('ep', 'tp'), may hold values from -600 to 600
- key_rows: bfloat16 [4096, 128], P('ep'), may hold values from -6 to 6
- value_rows: bfloat16 [4096, 128], P('ep'), may hold values from -48 to 48
- sink_logits: float32 [16], P('tp'), may hold values from 2 to 6
- out_weight: bfloat16 [1024, 2048], P('tp'), may hold values from -0.1875 to 0.1875
- moe_rows: bfloat16 [1024, 2048], P(('ep', 'tp')), may hold values from -6 to 6
- moe_gain: float32 [2048], replicated, may hold values from 0.1 to 1.9
- routes: int32 [1024, 2], P(('ep', 'tp')), may hold values from 0 to 3, all different within a row; in each aligned block of 32 rows (0 to 31, 32 to 63, ...) at most 24 rows name the same one
- route_weight: float32 [1024, 2], P(('ep', 'tp')), may hold values from 0.2 to 1
- gate_weight: bfloat16 [4, 2048, 7168], P('ep', None, 'tp'), may hold values from -0.125 to 0.125
- up_weight: bfloat16 [4, 2048, 7168], P('ep', None, 'tp'), may hold values from -0.125 to 0.125
- down_weight: bfloat16 [4, 7168, 2048], P('ep', 'tp'), may hold values from -0.0625 to 0.0625
Outputs:
- mixer_out: bfloat16 [4096, 2048], P(('ep', 'tp'))
- moe_out: bfloat16 [1024, 2048], P(('ep', 'tp'))
Inputs may be any that keep to these rules, and one draw needn't show every extreme that they name: `routes`: in each aligned block of 32 rows (the rows of one device) no expert is named more than 24 times, a bound that some block reaches; each row names 2 different experts.
All inputs are finite; a program needn't handle non-finite values.
Results may differ from a plain program's by a relative error of at most 0.02.
Values may be sent and summed in bfloat16 or wider, within the bound.
No kernel may reach another device: no remote copies, remote signals or barrier semaphores. Data moves between devices by JAX's collectives and lax.ppermute only.
A program may use at most 128 MiB of HBM per device.

v0:
```python
import jax
import jax.numpy as jnp
from jax import lax
from jax.sharding import PartitionSpec as P

HEADS = 16
KV_HEADS = 2
HEAD_DIM = 64
WINDOW = 128
TOP = 2


big_negative = -1e30
norm_eps = 1e-05


def passed_along(value, axis, steps):
    count = lax.axis_size(axis)
    initial, last = (max(0, -steps), min(count, count - steps))
    return lax.ppermute(value, axis, [(source, source + steps) for source in range(initial, last)])


def layer_normed(inputs, gain):
    values = inputs.astype(jnp.float32)
    center = values - jnp.mean(values, -1, keepdims=True)
    spread = jnp.mean(center * center, -1, keepdims=True)
    return (center * lax.rsqrt(spread + norm_eps) * gain).astype(jnp.bfloat16)


def attend(queries, key_rows, value_rows, sink_logits):
    total = queries.shape[0]
    heads_here = sink_logits.shape[0]
    blocks = total // WINDOW
    key_head = lax.axis_index("tp") * heads_here // (HEADS // KV_HEADS)
    key_own = lax.dynamic_slice_in_dim(key_rows, key_head * HEAD_DIM, HEAD_DIM, 1)
    value_own = lax.dynamic_slice_in_dim(value_rows, key_head * HEAD_DIM, HEAD_DIM, 1)
    last_rows = jnp.concatenate([key_own[total - WINDOW :], value_own[total - WINDOW :]], 1)
    earlier = passed_along(last_rows, "ep", 1)
    key_ext = jnp.concatenate([earlier[:, :HEAD_DIM], key_own], 0)
    value_ext = jnp.concatenate([earlier[:, HEAD_DIM:], value_own], 0)
    key_blocks = jnp.concatenate(
        [
            key_ext[:total].reshape(blocks, WINDOW, HEAD_DIM),
            key_ext[WINDOW:].reshape(blocks, WINDOW, HEAD_DIM),
        ],
        1,
    )
    value_blocks = jnp.concatenate(
        [
            value_ext[:total].reshape(blocks, WINDOW, HEAD_DIM),
            value_ext[WINDOW:].reshape(blocks, WINDOW, HEAD_DIM),
        ],
        1,
    )
    query_blocks = queries.reshape(blocks, WINDOW, heads_here, HEAD_DIM)
    scores = jnp.einsum(
        "nqhd,nkd->nhqk", query_blocks, key_blocks, preferred_element_type=jnp.float32
    ) * HEAD_DIM ** (-0.5)
    anchor = lax.axis_index("ep") * total
    block_base = anchor + jnp.arange(blocks, dtype=jnp.int32)[:, None, None] * WINDOW
    query_pos = block_base + jnp.arange(WINDOW, dtype=jnp.int32)[None, :, None]
    key_pos = block_base - WINDOW + jnp.arange(2 * WINDOW, dtype=jnp.int32)[None, None, :]
    allowed = ((key_pos <= query_pos) & (key_pos > query_pos - WINDOW) & (key_pos >= 0))[:, None]
    masked = jnp.where(allowed, scores, big_negative)
    sinks = sink_logits[None, :, None]
    row_max = jnp.maximum(jnp.max(masked, -1), sinks)
    powers = jnp.where(allowed, jnp.exp(masked - row_max[..., None]), 0.0)
    totals = jnp.sum(powers, -1) + jnp.exp(sinks - row_max)
    attn_probs = (powers / totals[..., None]).astype(jnp.bfloat16)
    attended = jnp.einsum(
        "nhqk,nkd->nqhd", attn_probs, value_blocks, preferred_element_type=jnp.float32
    )
    return attended.astype(jnp.bfloat16).reshape(total, heads_here * HEAD_DIM)


def mixer(queries, key_rows, value_rows, sink_logits, out_weight):
    attended = attend(queries, key_rows, value_rows, sink_logits)
    return lax.psum_scatter(
        jnp.dot(attended, out_weight, preferred_element_type=jnp.float32).astype(jnp.bfloat16),
        "tp",
        scatter_dimension=0,
        tiled=True,
    )


def experts(moe_rows, moe_gain, routes, route_weight, gate_weight, up_weight, down_weight):
    row_count = moe_rows.shape[0]
    width_all = moe_rows.shape[1]
    expert_count = gate_weight.shape[0] * lax.axis_size("ep")
    capacity = 3 * row_count * TOP // (2 * expert_count)
    normed = layer_normed(moe_rows, moe_gain)
    chosen = routes.reshape(-1)
    onehot = (chosen[:, None] == jnp.arange(expert_count, dtype=jnp.int32)[None, :]).astype(
        jnp.int32
    )
    earlier_count = jnp.cumsum(onehot, 0) - onehot
    slot_index = jnp.sum(earlier_count * onehot, 1)
    target = chosen * capacity + slot_index
    matches = target[None, :] == jnp.arange(expert_count * capacity, dtype=jnp.int32)[:, None]
    dispatch_map = jnp.sum(matches.reshape(expert_count * capacity, row_count, TOP), -1).astype(
        jnp.bfloat16
    )
    buffer = jnp.dot(dispatch_map, normed, preferred_element_type=jnp.float32).astype(jnp.bfloat16)
    buffer = buffer.reshape(expert_count, capacity, width_all)
    gate_mat = gate_weight[0]
    up_mat = up_weight[0]
    down_mat = down_weight[0]
    received = lax.all_to_all(buffer, "ep", split_axis=0, concat_axis=0, tiled=True)
    total = received.shape[0] * received.shape[1]
    flat_rows = received.reshape(total, width_all)
    shard_rows = lax.all_gather(flat_rows, "tp", axis=0, tiled=True)
    gate_val = jnp.dot(shard_rows, gate_mat, preferred_element_type=jnp.float32)
    up_val = jnp.dot(shard_rows, up_mat, preferred_element_type=jnp.float32)
    hidden = (jax.nn.silu(gate_val) * up_val).astype(jnp.bfloat16)
    summed = lax.psum_scatter(
        jnp.dot(hidden, down_mat, preferred_element_type=jnp.float32).astype(jnp.bfloat16),
        "tp",
        scatter_dimension=0,
        tiled=True,
    )
    results = summed.reshape(received.shape)
    returned = lax.all_to_all(results, "ep", split_axis=0, concat_axis=0, tiled=True)
    weights_flat = route_weight.reshape(-1)
    combine_map = jnp.sum(
        jnp.where(matches, weights_flat[None, :], 0.0).reshape(
            expert_count * capacity, row_count, TOP
        ),
        -1,
    )
    returned_flat = returned.reshape(expert_count * capacity, width_all).astype(jnp.float32)
    moe_out = lax.dot_general(
        combine_map, returned_flat, (((0,), (0,)), ((), ())), precision=lax.Precision.HIGHEST
    )
    return moe_out.astype(jnp.bfloat16)


def body(
    queries,
    key_rows,
    value_rows,
    sink_logits,
    out_weight,
    moe_rows,
    moe_gain,
    routes,
    route_weight,
    gate_weight,
    up_weight,
    down_weight,
):
    mixer_out = mixer(queries, key_rows, value_rows, sink_logits, out_weight)
    moe_out = experts(moe_rows, moe_gain, routes, route_weight, gate_weight, up_weight, down_weight)
    return (mixer_out, moe_out)


def solution(mesh):
    in_specs = (
        P("ep", "tp"),
        P("ep", None),
        P("ep", None),
        P("tp"),
        P("tp", None),
        P(("ep", "tp"), None),
        P(),
        P(("ep", "tp"), None),
        P(("ep", "tp"), None),
        P("ep", None, "tp"),
        P("ep", None, "tp"),
        P("ep", "tp", None),
    )
    out_specs = (P(("ep", "tp"), None), P(("ep", "tp"), None))
    return jax.shard_map(body, mesh=mesh, in_specs=in_specs, out_specs=out_specs, check_vma=False)
```

profile of v0, /device:TPU:0, one launch (start us, length us, event | category | flops | bytes accessed | tf_op | source)
XLA Modules:
  0.0 179.6 jit_solution(15246932592447311926)
XLA Ops:
  7.2 1.1 convert_reduce_fusion
  8.3 1.1 fusion.20
  9.4 0.8 copy.64
  10.5 0.2 select_reduce_fusion.1
  10.9 0.7 multiply_add_fusion
  11.6 1.2 convolution_convert_fusion.1
  12.9 12.2 %all_to_all.10 = bf16[4,24,2048]{2,1,0:T(8,128)(2,1)} all-to-all(bf16[4,24,2048]{2,1,0:T(8,128)(2,1)S(1)} %bitcast.65), channel_id=1, replica_groups=mesh['ep'=4,'tp'=8] {'ep'}, dimensions={0} | all-to-all | bytes 786432 | tf_op jit(solution)/shard_map/all_to_all | solution.py:108
  25.2 38.0 %all-gather.2.cloned.1.call-done = bf16[768,2048]{1,0:T(8,128)(2,1)} async-done(((bf16[96,2048]{1,0:T(8,128)(2,1)}), bf16[768,2048]{1,0:T(8,128)(2,1)}) %all-gather.2.cloned.1.call-update) | async-done | bytes 3145744 | tf_op jit(solution)/shard_map/all_gather | solution.py:111
  63.2 6.4 %fusion.2 = f32[768,896]{1,0:T(8,128)S(1)} fusion(bf16[768,2048]{1,0:T(8,128)(2,1)} %all-gather.2.cloned.1.call-done, bf16[1,2048,896]{2,1,0:T(8,128)(2,1)} %param.22), kind=kOutput, calls=%fused_computation.3 | convolution fusion | flops 2818572288 | bytes 9568256 | tf_op jit(solution)/shard_map/dot_general | solution.py:113
  69.6 11.8 %fusion.6 = bf16[768,2048]{1,0:T(8,128)(2,1)} fusion(bf16[1,896,2048]{2,1,0:T(8,128)(2,1)} %param.23, f32[768,896]{1,0:T(8,128)S(1)} %fusion.2, bf16[768,2048]{1,0:T(8,128)(2,1)} %all-gather.2.cloned.1.call-done, bf16[1,2048,896]{2,1,0:T(8,128)(2,1)} %param.21), kind=kOutput, calls=%fused_computation.7 | convolution fusion | flops 5642846208 | bytes 16384000 | tf_op jit(solution)/shard_map/dot_general | solution.py:116
  81.5 0.8 copy-done.2
  82.7 3.4 %collective-permute-start = (bf16[128,128]{1,0:T(8,128)(2,1)S(1)}, bf16[128,128]{1,0:T(8,128)(2,1)S(1)}, u32[]{:S(2)}, u32[]{:S(2)}) collective-permute-start(bf16[128,128]{1,0:T(8,128)(2,1)S(1)} %pad_maximum_fusion.2), channel_id=1, source_target_pairs={{0,8},{8,16},{16,24},{1,9},{9,17},{17,25},{2,10},{10,18},{18,26},{... | collective-permute-start | bytes 98312 | tf_op jit(solution)/shard_map/ppermute | solution.py:20
  86.3 0.7 and_and_fusion
  87.0 0.2 constant_dynamic-slice_fusion
  87.5 0.2 reshape.202
  88.3 0.6 fusion.11
  88.9 0.6 fusion.12
  89.6 0.7 fusion.13
  90.5 3.2 %convolution_convert_fusion = bf16[1024,2048]{1,0:T(8,128)(2,1)} fusion(bf16[128,2048]{1,0:T(8,128)(2,1)S(1)} %copy-done, bf16[16,8,8,128]{3,2,1,0:T(8,128)(2,1)S(1)} %bitcast.62), kind=kOutput, calls=%fused_computation | convolution fusion | flops 538968064 | bytes 4980736 | tf_op jit(solution)/shard_map/dot_general | solution.py:79
  93.8 27.1 %reduce-scatter.5.cloned.1.call-done = bf16[96,2048]{1,0:T(8,128)(2,1)} async-done(((bf16[768,2048]{1,0:T(8,128)(2,1)}), bf16[96,2048]{1,0:T(8,128)(2,1)}) %reduce-scatter.5.cloned.1.call-update) | async-done | bytes 393232 | tf_op jit(solution)/shard_map/reduce_scatter | solution.py:115
  120.9 3.7 %all-to-all-start.1 = ((bf16[4,24,2048]{2,1,0:T(8,128)(2,1)}), bf16[4,24,2048]{2,1,0:T(8,128)(2,1)S(1)}, u32[]{:S(2)}, u32[]{:S(2)}) async-start(bf16[4,24,2048]{2,1,0:T(8,128)(2,1)} %bitcast.68), calls=%async_computation.3 | async-start | bytes 786432 | tf_op jit(solution)/shard_map/all_to_all | solution.py:122
  124.7 5.8 %all-to-all-done.1 = bf16[4,24,2048]{2,1,0:T(8,128)(2,1)S(1)} async-done(((bf16[4,24,2048]{2,1,0:T(8,128)(2,1)}), bf16[4,24,2048]{2,1,0:T(8,128)(2,1)S(1)}, u32[]{:S(2)}, u32[]{:S(2)}) %all-to-all-start.1) | async-done | bytes 393248 | tf_op jit(solution)/shard_map/all_to_all | solution.py:122
  130.4 0.9 convolution_convert_fusion.2
  131.4 41.7 %reduce-scatter.3.cloned.1.call-done = bf16[128,2048]{1,0:T(8,128)(2,1)} async-done(((bf16[1024,2048]{1,0:T(8,128)(2,1)}), bf16[128,2048]{1,0:T(8,128)(2,1)}) %reduce-scatter.3.cloned.1.call-update) | async-done | bytes 524304 | tf_op jit(solution)/shard_map/reduce_scatter | solution.py:78
  (44 shorter events, 2.4 us)
Async XLA Ops:
  7.2 83.4 %copy-start = (bf16[128,2048]{1,0:T(8,128)(2,1)S(1)}, bf16[128,2048]{1,0:T(8,128)(2,1)}, u32[]{:S(2)}) copy-start(bf16[128,2048]{1,0:T(8,128)(2,1)} %param.16) | copy-start | bytes 1572868
  7.2 56.0 %all-gather.2.cloned.1.call-start = ((), (), s32[]{:S(2)}) async-start(), calls=%async_computation.5 | async-start | bytes 3538944 | tf_op jit(solution)/shard_map/all_gather | solution.py:111
  25.1 95.8 %reduce-scatter.5.cloned.1.call-start = ((), (), s32[]{:S(2)}) async-start(), calls=%async_computation.6 | async-start | bytes 3538944 | tf_op jit(solution)/shard_map/reduce_scatter | solution.py:115
  81.4 0.9 copy-start.2
  81.4 1.0 copy-start.1
  81.4 6.1 %copy-start.3 = (bf16[1024,128]{1,0:T(8,128)(2,1)S(1)}, bf16[1024,128]{1,0:T(8,128)(2,1)}, u32[]{:S(2)}) copy-start(bf16[1024,128]{1,0:T(8,128)(2,1)} %param.12) | copy-start | bytes 786436
  81.5 91.6 %reduce-scatter.3.cloned.1.call-start = ((), (), s32[]{:S(2)}) async-start(), calls=%async_computation.4 | async-start | bytes 4718592 | tf_op jit(solution)/shard_map/reduce_scatter | solution.py:78
  82.7 5.1 %collective-permute-start = (bf16[128,128]{1,0:T(8,128)(2,1)S(1)}, bf16[128,128]{1,0:T(8,128)(2,1)S(1)}, u32[]{:S(2)}, u32[]{:S(2)}) collective-permute-start(bf16[128,128]{1,0:T(8,128)(2,1)S(1)} %pad_maximum_fusion.2), channel_id=1, source_target_pairs={{0,8},{8,16},{16,24},{1,9},{9,17},{17,25},{2,10},{10,18},{18,26},{... | collective-permute-start | bytes 98312 | tf_op jit(solution)/shard_map/ppermute | solution.py:20
  87.8 1.1 copy-start.4
  93.7 30.8 %copy-start.5 = (f32[32,2]{0,1:T(2,128)S(1)}, f32[32,2]{0,1:T(2,128)}, u32[]{:S(2)}) copy-start(f32[32,2]{0,1:T(2,128)} %param.20) | copy-start | bytes 772
  120.9 9.5 %all-to-all-start.1 = ((bf16[4,24,2048]{2,1,0:T(8,128)(2,1)}), bf16[4,24,2048]{2,1,0:T(8,128)(2,1)S(1)}, u32[]{:S(2)}, u32[]{:S(2)}) async-start(bf16[4,24,2048]{2,1,0:T(8,128)(2,1)} %bitcast.68), calls=%async_computation.3 | async-start | bytes 786432 | tf_op jit(solution)/shard_map/all_to_all | solution.py:122
Sparse Core Ops, SparseCore 0:
  25.2 37.9 all-gather.1
  81.6 39.2 reduce-scatter.4
  123.8 49.2 reduce-scatter.2
where the time goes:
time: 180 us
  waiting for transfers between devices  113 us (63%)
  matrix products  24.9 us (14%)
  between operations  14 us (8%)
  blocking collectives  12.2 us (7%)
  starting transfers between devices  7.15 us (4%)
  other arithmetic  5.28 us (3%)
  local copies, waits for them, and re-layouts  3.39 us (2%)
    reduce_scatter x1, waiting for transfers between devices, mixer(): lax.psum_scatter(jnp.dot(attended, out_weight, preferred_element_type=jnp...  41.7 us
    all_gather x1, waiting for transfers between devices, experts(): shard_rows = lax.all_gather(flat_rows, 'tp', axis=0, tiled=True)  38 us
    reduce_scatter x1, waiting for transfers between devices, experts(): lax.psum_scatter(jnp.dot(hidden, down_mat, preferred_element_type=jnp.flo...  27.1 us
    all_to_all x1, blocking collectives, experts(): lax.all_to_all(buffer, 'ep', split_axis=0, concat_axis=0, tiled=True)  12.2 us
    dot_general x1, matrix products, experts(): jnp.dot(hidden, down_mat, preferred_element_type=jnp.float32)  11.8 us
    dot_general x1, matrix products, experts(): up_val = jnp.dot(shard_rows, up_mat, preferred_element_type=jnp.float32)  6.39 us
    all_to_all x1, waiting for transfers between devices, experts(): lax.all_to_all(results, 'ep', split_axis=0, concat_axis=0, tiled=True)  5.79 us
    all_to_all x1, starting transfers between devices, experts(): lax.all_to_all(results, 'ep', split_axis=0, concat_axis=0, tiled=True)  3.65 us
  transfers between devices with their start and end apart: 5, of which 4 were waited for; matrix products, arithmetic and copies ran while one was open for 5% of the time, Pallas kernels for 0%

commit v1 on v0

v1 whole, which is shorter than its diff:
```python
import functools

import jax
import jax.numpy as jnp
from jax import lax
from jax.experimental import pallas as pl
from jax.experimental.pallas import tpu as pltpu
from jax.sharding import PartitionSpec as P


HEADS = 16
KV_HEADS = 2
HEAD_DIM = 64
WINDOW = 128
TOP = 2
CORES = 2


big_negative = -1e30
norm_eps = 1e-05
BF = jnp.bfloat16
F32 = jnp.float32
VMEM = pl.BlockSpec(memory_space=pltpu.VMEM)
SMEM = pl.BlockSpec(memory_space=pltpu.SMEM)
HBM = pl.BlockSpec(memory_space=pltpu.HBM)


def swapped(value, axis, mask):
    count = lax.axis_size(axis)
    return lax.ppermute(value, axis, [(i, i ^ mask) for i in range(count)])


def small(mib):
    return pltpu.CompilerParams(vmem_limit_bytes=mib << 20)


def fetch(sources, targets, sems):
    copies = [pltpu.make_async_copy(s, t, sems.at[i]) for i, (s, t) in enumerate(zip(sources, targets))]
    for copy in copies:
        copy.start()
    return copies


def cost(flops, moved):
    return pl.CostEstimate(flops=int(flops), bytes_accessed=int(moved), transcendentals=0)


def nt(a, b):
    return lax.dot_general(a, b, (((1,), (1,)), ((), ())), preferred_element_type=F32)


def relative(i, groups_z):
    far, core, k = i // (2 * groups_z), (i // groups_z) % 2, i % groups_z
    return far * (2 * groups_z) + 2 * k + core


def attend_kernel(where_ref, sink_ref, q_hbm, k_hbm, v_hbm, early_ref, *refs):
    out_refs, (q_ref, k_ref, v_ref, sems) = refs[:4], refs[4:]
    for copy in fetch((q_hbm, k_hbm, v_hbm), (q_ref, k_ref, v_ref), sems):
        copy.wait()
    blocks = q_ref.shape[0] // WINDOW
    heads_here = q_ref.shape[1] // HEAD_DIM
    groups_z = blocks // 4
    key_head = where_ref[1]
    width = KV_HEADS * HEAD_DIM

    def own(values):
        parts = [values[:, h * HEAD_DIM : (h + 1) * HEAD_DIM] for h in range(KV_HEADS)]
        picked = parts[0]
        for h in range(1, KV_HEADS):
            picked = jnp.where(key_head == h, parts[h], picked)
        return picked

    row = lax.broadcasted_iota(jnp.int32, (WINDOW, WINDOW), 0)
    col = lax.broadcasted_iota(jnp.int32, (WINDOW, WINDOW), 1)
    cur_ok = col <= row
    for i in range(blocks):
        block = where_ref[0] ^ relative(i, groups_z)
        first = block == 0
        no_past = jnp.logical_and(first, where_ref[2] == 0)
        here = pl.ds(pl.multiple_of(block * WINDOW, WINDOW), WINDOW)
        past = pl.ds(pl.multiple_of(jnp.maximum(block - 1, 0) * WINDOW, WINDOW), WINDOW)
        k_cur, v_cur = own(k_ref[here, :]), own(v_ref[here, :])
        k_past = own(jnp.where(first, early_ref[:, :width], k_ref[past, :]))
        v_past = own(jnp.where(first, early_ref[:, width:], v_ref[past, :]))
        past_ok = jnp.logical_and(col > row, jnp.logical_not(no_past))
        out_ref, place = out_refs[i // groups_z], (i % groups_z) * WINDOW
        for h in range(heads_here):
            cols = slice(h * HEAD_DIM, (h + 1) * HEAD_DIM)
            q = q_ref[here, cols]
            sink = sink_ref[h]
            s_past = jnp.where(past_ok, nt(q, k_past) * HEAD_DIM ** (-0.5), big_negative)
            s_cur = jnp.where(cur_ok, nt(q, k_cur) * HEAD_DIM ** (-0.5), big_negative)
            top = jnp.maximum(jnp.max(jnp.maximum(s_past, s_cur), -1, keepdims=True), sink)
            e_past = jnp.where(past_ok, jnp.exp(s_past - top), 0.0)
            e_cur = jnp.where(cur_ok, jnp.exp(s_cur - top), 0.0)
            total = jnp.sum(e_past + e_cur, -1, keepdims=True) + jnp.exp(sink - top)
            scale = 1.0 / total
            mixed = jnp.dot((e_past * scale).astype(BF), v_past, preferred_element_type=F32)
            mixed += jnp.dot((e_cur * scale).astype(BF), v_cur, preferred_element_type=F32)
            out_ref[place : place + WINDOW, cols] = mixed.astype(BF)


def attend(queries, key_rows, value_rows, sink_logits, earlier):
    total, cols = queries.shape
    assert total // lax.axis_size("tp") == WINDOW
    tp = lax.axis_index("tp")
    key_head = tp * sink_logits.shape[0] // (HEADS // KV_HEADS)
    place = jnp.stack([tp, key_head, lax.axis_index("ep")]).astype(jnp.int32)
    return pl.pallas_call(
        attend_kernel,
        in_specs=[SMEM, SMEM] + [HBM] * 3 + [VMEM],
        out_specs=[VMEM] * 4,
        out_shape=[jax.ShapeDtypeStruct((total // 4, cols), BF)] * 4,
        scratch_shapes=[pltpu.VMEM(a.shape, BF) for a in (queries, key_rows, value_rows)]
        + [pltpu.SemaphoreType.DMA((3,))],
        cost_estimate=cost(4e9, 2e6),
        compiler_params=small(8),
        name="attend",
    )(place, sink_logits, queries, key_rows, value_rows, earlier)


def project_kernel(count, *refs):
    parts, mats, outs = refs[:count], refs[count : 2 * count], refs[2 * count :]
    rows = outs[0].shape[0]
    width = mats[0].shape[1]
    tile = min(512, width)
    for n in range(0, width, tile):
        total = None
        for part, mat in zip(parts, mats):
            term = jnp.dot(part[...], mat[:, n : n + tile], preferred_element_type=F32)
            total = term if total is None else total + term
        for i, out in enumerate(outs):
            out[:, n : n + tile] = total[i * rows : (i + 1) * rows].astype(out.dtype)


def project(parts, mats):
    rows = parts[0].shape[0]
    width = mats[0].shape[1]
    groups = rows // WINDOW
    out = [jax.ShapeDtypeStruct((WINDOW, width), F32 if i == 0 else BF) for i in range(groups)]
    return pl.pallas_call(
        functools.partial(project_kernel, len(parts)),
        in_specs=[VMEM] * (2 * len(parts)),
        out_specs=[VMEM] * groups,
        out_shape=out,
        cost_estimate=cost(2e9, 4e6),
        compiler_params=small(12),
        name="project",
    )(*parts, *mats)


def norm_kernel(experts, *refs):
    sources, (out_ref, last_ref), targets, sems = refs[:6], refs[6:8], refs[8:14], refs[14]
    x_ref, gain_ref, routes_ref, weight_ref, k_ref, v_ref = targets
    end = pl.ds(sources[4].shape[0] - WINDOW, WINDOW)
    copies = fetch(sources[:4] + (sources[4].at[end], sources[5].at[end]), targets, sems)
    for copy in copies:
        copy.wait()
    width = x_ref.shape[1]
    values = x_ref[...].astype(F32)
    center = values - jnp.mean(values, -1, keepdims=True)
    spread = jnp.mean(center * center, -1, keepdims=True)
    out_ref[:, :width] = (center * lax.rsqrt(spread + norm_eps) * gain_ref[...]).astype(BF)
    lane = lax.broadcasted_iota(jnp.int32, (128, x_ref.shape[0]), 0)
    expert = jnp.where(lane < experts, lane, lane - experts)
    weight = jnp.zeros(lane.shape, F32)
    for k in range(TOP):
        weight += jnp.where(routes_ref[k : k + 1, :] == expert, weight_ref[k : k + 1, :], 0.0)
    high = weight.astype(BF).astype(F32)
    table = jnp.where(lane < experts, high, jnp.where(lane < 2 * experts, weight - high, 0.0))
    out_ref[:, width:] = table.T.astype(BF)
    last_ref[:, : k_ref.shape[1]] = k_ref[...]
    last_ref[:, k_ref.shape[1] :] = v_ref[...]


def normed_rows(moe_rows, moe_gain, routes, route_weight, experts, key_rows, value_rows):
    rows, width = moe_rows.shape
    cols = key_rows.shape[1]
    args = (moe_rows, moe_gain[None, :], routes.T, route_weight.T, key_rows, value_rows)
    shapes = [a.shape for a in args[:4]] + [(WINDOW, cols)] * 2
    return pl.pallas_call(
        functools.partial(norm_kernel, experts),
        in_specs=[HBM] * 6,
        out_specs=[VMEM] * 2,
        out_shape=[
            jax.ShapeDtypeStruct((rows, width + 128), BF),
            jax.ShapeDtypeStruct((WINDOW, 2 * cols), BF),
        ],
        scratch_shapes=[pltpu.VMEM(shape, a.dtype) for shape, a in zip(shapes, args)]
        + [pltpu.SemaphoreType.DMA((6,))],
        cost_estimate=cost(1e7, 3e5),
        compiler_params=small(8),
        name="normed",
    )(*args)


def slots_of(experts, capacity, blocks, width):
    rows = blocks[0].shape[0]
    tokens = rows * len(blocks)
    table = jnp.concatenate([b[:, width:] for b in blocks], 0).astype(F32).T
    flags = (table > 0).astype(BF)
    source = lax.broadcasted_iota(jnp.int32, (tokens, tokens), 0)
    target = lax.broadcasted_iota(jnp.int32, (tokens, tokens), 1)
    ahead = jnp.logical_and(source < target, source // rows == target // rows).astype(BF)
    position = jnp.dot(flags, ahead, preferred_element_type=F32)
    lane = lax.broadcasted_iota(jnp.int32, (128, tokens), 0)
    base = (lax.broadcasted_iota(jnp.int32, (1, tokens), 1) // rows) * capacity

    def of(expert):
        high = jnp.sum(jnp.where(lane == expert, table, 0.0), 0, keepdims=True)
        low = jnp.sum(jnp.where(lane == expert + experts, table, 0.0), 0, keepdims=True)
        place = jnp.sum(jnp.where(lane == expert, position, 0.0), 0, keepdims=True)
        return jnp.where(high > 0, base + place.astype(jnp.int32), -1), high, low

    return of


def pick_kernel(experts, capacity, ep_ref, *refs):
    lines = len(refs) - experts
    blocks, picked = refs[:lines], refs[lines:]
    slots, width = picked[0].shape
    of = slots_of(experts, capacity, blocks, width)
    slot_id = lax.broadcasted_iota(jnp.int32, (slots, blocks[0].shape[0] * lines), 0)
    values = jnp.concatenate([b[:, :width] for b in blocks], 0)
    for k in range(experts):
        hit = (slot_id == of(ep_ref[0] ^ k)[0]).astype(BF)
        picked[k][...] = jnp.dot(hit, values, preferred_element_type=F32).astype(BF)


def maps_kernel(experts, capacity, ep_ref, *refs):
    lines = len(refs) - 1
    blocks, maps_ref = refs[:lines], refs[lines]
    slots = capacity * lines
    of = slots_of(experts, capacity, blocks, 0)
    slot_id = lax.broadcasted_iota(jnp.int32, (slots, blocks[0].shape[0] * lines), 0)
    for k in range(experts):
        slot, high, low = of(ep_ref[0] ^ k)
        hit = slot_id == slot
        for j, part in enumerate((high, low)):
            maps_ref[2 * k + j] = jnp.where(hit, part, 0.0).T.astype(BF)


def pick(blocks, experts, capacity):
    _, width = blocks[0].shape
    width -= 128
    slots = capacity * len(blocks)
    ep = lax.axis_index("ep").astype(jnp.int32)[None]
    return pl.pallas_call(
        functools.partial(pick_kernel, experts, capacity),
        in_specs=[SMEM] + [VMEM] * len(blocks),
        out_specs=[VMEM] * experts,
        out_shape=[jax.ShapeDtypeStruct((slots, width), BF)] * experts,
        cost_estimate=cost(2e8, 2e6),
        compiler_params=small(12),
        name="pick",
    )(ep, *blocks)


def weight_maps(blocks, experts, capacity):
    rows, width = blocks[0].shape
    slots, tokens = capacity * len(blocks), rows * len(blocks)
    ep = lax.axis_index("ep").astype(jnp.int32)[None]
    tail = pl.BlockSpec((rows, 128), lambda i: (0, width // 128 - 1))
    return pl.pallas_call(
        functools.partial(maps_kernel, experts, capacity),
        grid=(1,),
        in_specs=[SMEM] + [tail] * len(blocks),
        out_specs=pl.BlockSpec((2 * experts, tokens, slots), lambda i: (0, 0, 0)),
        out_shape=jax.ShapeDtypeStruct((2 * experts, tokens, slots), BF),
        cost_estimate=cost(2e7, 1e6),
        compiler_params=small(12),
        name="maps",
    )(ep, *blocks)


def expert_kernel(count, *refs):
    rows_refs = refs[:count]
    own_mats, other_mats = refs[count : count + 3], refs[count + 3 : count + 6]
    outs = refs[count + 6 : 2 * count + 6]
    all_rows, hidden, sems = refs[2 * count + 6 : 2 * count + 9]
    held = refs[2 * count + 9 :]
    copies = fetch(other_mats, held, sems)
    gates, ups, downs = zip(own_mats, held)
    slots, width = rows_refs[0].shape
    units = gates[0].shape[1]
    for i in range(count):
        all_rows[i * slots : (i + 1) * slots, :] = rows_refs[i][...]
    tile = 256
    for j in range(2):
        if j == 1:
            copies[0].wait()
            copies[1].wait()
        for n in range(0, units, tile):
            cols = slice(n, min(n + tile, units))
            g = jnp.dot(all_rows[...], gates[j][:, cols], preferred_element_type=F32)
            u = jnp.dot(all_rows[...], ups[j][:, cols], preferred_element_type=F32)
            hidden[j, :, cols] = (g / (1.0 + jnp.exp(-g)) * u).astype(BF)
    copies[2].wait()
    for n in range(0, width, tile):
        cols = slice(n, n + tile)
        total = jnp.dot(hidden[0], downs[0][:, cols], preferred_element_type=F32)
        total += jnp.dot(hidden[1], downs[1][:, cols], preferred_element_type=F32)
        for i in range(count):
            outs[i][:, cols] = total[i * slots : (i + 1) * slots].astype(BF)


def expert(row_sets, own_mats, other_mats):
    count = len(row_sets)
    slots, width = row_sets[0].shape
    units = own_mats[0].shape[1]
    total = count * slots
    return pl.pallas_call(
        functools.partial(expert_kernel, count),
        in_specs=[VMEM] * (count + 3) + [HBM] * 3,
        out_specs=[VMEM] * count,
        out_shape=[jax.ShapeDtypeStruct((slots, width), BF)] * count,
        scratch_shapes=[
            pltpu.VMEM((total, width), BF),
            pltpu.VMEM((2, total, units), BF),
            pltpu.SemaphoreType.DMA((3,)),
        ]
        + [pltpu.VMEM(m.shape, BF) for m in other_mats],
        cost_estimate=cost(12 * total * width * units, 12 * width * units),
        compiler_params=small(22),
        name="expert",
    )(*row_sets, *own_mats, *other_mats)


def combine_kernel(experts, maps_ref, *refs):
    results, outs = refs[:experts], refs[experts:]
    rows, width = outs[0].shape
    tile = min(512, width)
    for n in range(0, width, tile):
        cols = slice(n, n + tile)
        total = None
        for k in range(experts):
            for j in range(2):
                term = jnp.dot(maps_ref[2 * k + j], results[k][:, cols], preferred_element_type=F32)
                total = term if total is None else total + term
        for i, out in enumerate(outs):
            out[:, cols] = total[i * rows : (i + 1) * rows].astype(out.dtype)


def combine(maps, results, lines):
    experts = len(results)
    width = results[0].shape[1]
    rows = maps.shape[1] // lines
    out = [jax.ShapeDtypeStruct((rows, width), F32 if i == 0 else BF) for i in range(lines)]
    return pl.pallas_call(
        functools.partial(combine_kernel, experts),
        in_specs=[VMEM] * (1 + experts),
        out_specs=[VMEM] * lines,
        out_shape=out,
        cost_estimate=cost(5e8, 3e6),
        compiler_params=small(12),
        name="combine",
    )(maps, *results)


def body(
    queries,
    key_rows,
    value_rows,
    sink_logits,
    out_weight,
    moe_rows,
    moe_gain,
    routes,
    route_weight,
    gate_weight,
    up_weight,
    down_weight,
):
    tp, ep = lax.axis_size("tp"), lax.axis_size("ep")
    lines, far = tp // CORES, tp // 2
    experts_all = gate_weight.shape[0] * ep
    capacity = 3 * moe_rows.shape[0] * TOP // (2 * experts_all)

    own_mats = (gate_weight[0], up_weight[0], down_weight[0])
    other_mats = [swapped(m, "tp", 1) for m in own_mats]

    own, last = normed_rows(
        moe_rows, moe_gain, routes, route_weight, experts_all, key_rows, value_rows
    )
    blocks = [own] + [swapped(own, "tp", CORES * k) for k in range(1, lines)]
    earlier = lax.ppermute(last, "ep", [(i, i + 1) for i in range(ep - 1)])

    picked = pick(blocks, experts_all, capacity)
    arrived = [picked[0]] + [swapped(picked[k], "ep", k) for k in range(1, ep)]
    maps = weight_maps(blocks, experts_all, capacity)

    pieces = attend(queries, key_rows, value_rows, sink_logits, earlier)
    parts = [pieces[0]] + [
        swapped(pieces[i], "tp", mask)
        for i, mask in ((1, 1), (2, far), (3, far + 1))
    ]
    far_weight = swapped(out_weight, "tp", far)
    mats = [out_weight, swapped(out_weight, "tp", 1), far_weight, swapped(far_weight, "tp", 1)]
    shares = project(parts, mats)
    mixer = shares[0]
    for k in range(1, far // CORES):
        mixer += swapped(shares[k], "tp", CORES * k).astype(F32)

    order = list(range(1, ep)) + [0]
    results = [None] * ep
    for group in (order[: ep // 2], order[ep // 2 :]):
        done = expert([arrived[k] for k in group], own_mats, other_mats)
        for k, value in zip(group, done):
            results[k] = value
    returned = [results[0]] + [swapped(results[k], "ep", k) for k in range(1, ep)]

    sums = combine(maps, returned, lines)
    moe = sums[0]
    for k in range(1, lines):
        moe += swapped(sums[k], "tp", CORES * k).astype(F32)
    return (mixer.astype(BF), moe.astype(BF))


def solution(mesh):
    in_specs = (
        P("ep", "tp"),
        P("ep", None),
        P("ep", None),
        P("tp"),
        P("tp", None),
        P(("ep", "tp"), None),
        P(),
        P(("ep", "tp"), None),
        P(("ep", "tp"), None),
        P("ep", None, "tp"),
        P("ep", None, "tp"),
        P("ep", "tp", None),
    )
    out_specs = (P(("ep", "tp"), None), P(("ep", "tp"), None))
    return jax.shard_map(body, mesh=mesh, in_specs=in_specs, out_specs=out_specs, check_vma=False)
```

time: 180 us -> 137 us (0.76)
  waiting for transfers between devices: 113 us -> 64.4 us
  Pallas kernels: 0 us -> 28.1 us
  starting transfers between devices: 7.15 us -> 33.5 us
  matrix products: 24.9 us -> 0 us
  between operations: 14 us -> 0.8 us
  blocking collectives: 12.2 us -> 0 us
  local copies, waits for them, and re-layouts: 3.39 us -> 8.37 us
  other arithmetic: 5.28 us -> 1.69 us
    reduce_scatter x2 -> x0, waiting for transfers between devices: 68.8 us -> none  [the longest x1 41.7 us: mixer(): lax.psum_scatter(jnp.dot(attended, out_weight, preferred_element_type=jnp...]
    ppermute x1 -> x23, waiting for transfers between devices: 0.01 us -> 64.4 us  [the longest x22 62.6 us: swapped(): return lax.ppermute(value, axis, [(i, i ^ mask) for i in range(count)])]
    all_gather x1 -> x0, waiting for transfers between devices: 38 us -> none  [experts(): shard_rows = lax.all_gather(flat_rows, 'tp', axis=0, tiled=True)]
    ppermute x1 -> x23, starting transfers between devices: 3.38 us -> 33.5 us  [the longest x22 29 us: swapped(): return lax.ppermute(value, axis, [(i, i ^ mask) for i in range(count)])]
    pallas_call x0 -> x8, Pallas kernels: none -> 28.1 us  [the longest x2 17 us: expert(): pl.pallas_call(functools.partial(expert_kernel, count), in_specs=[VMEM] *...]
    dot_general x7 -> x0, matrix products: 24.9 us -> none  [the longest x1 11.8 us: experts(): jnp.dot(hidden, down_mat, preferred_element_type=jnp.float32)]
    all_to_all x1 -> x0, blocking collectives: 12.2 us -> none  [experts(): lax.all_to_all(buffer, 'ep', split_axis=0, concat_axis=0, tiled=True)]
    unnamed x13 -> x28, local copies, waits for them, and re-layouts: 1.65 us -> 8.37 us
  transfers between devices with their start and end apart: 5 -> 23, of which waited for: 4 -> 10; matrix products, arithmetic and copies ran while one was open for 5% -> 1% of each run, Pallas kernels for 0% -> 21%
where the time goes in v1:
time: 137 us
  waiting for transfers between devices  64.4 us (47%)
  starting transfers between devices  33.5 us (24%)
  Pallas kernels  28.1 us (21%)
  local copies, waits for them, and re-layouts  8.37 us (6%)
  other arithmetic  1.69 us (1%)
    ppermute x22, waiting for transfers between devices, swapped(): return lax.ppermute(value, axis, [(i, i ^ mask) for i in range(count)])  62.6 us
    ppermute x22, starting transfers between devices, swapped(): return lax.ppermute(value, axis, [(i, i ^ mask) for i in range(count)])  29 us
    pallas_call x2, Pallas kernels, expert(): pl.pallas_call(functools.partial(expert_kernel, count), in_specs=[VMEM] *...  17 us
    unnamed x28, local copies, waits for them, and re-layouts  8.37 us
    pallas_call x1, Pallas kernels, attend(): pl.pallas_call(attend_kernel, in_specs=[SMEM, SMEM] + [HBM] * 3 + [VMEM],...  6.89 us
    ppermute x1, starting transfers between devices, body(): earlier = lax.ppermute(last, 'ep', [(i, i + 1) for i in range(ep - 1)])  4.46 us
  transfers between devices with their start and end apart: 23, of which 10 were waited for; matrix products, arithmetic and copies ran while one was open for 1% of the time, Pallas kernels for 21%

profile of v1, /device:TPU:0, one launch (start us, length us, event | category | flops | bytes accessed | tf_op | source)
XLA Modules:
  0.0 136.9 jit_solution(5579010108293185595)
XLA Ops:
  7.1 4.5 %collective-permute-start = (bf16[128,256]{1,0:T(8,128)(2,1)S(1)}, bf16[128,256]{1,0:T(8,128)(2,1)S(1)}, u32[]{:S(2)}, u32[]{:S(2)}) collective-permute-start(bf16[128,256]{1,0:T(8,128)(2,1)S(1)} %get-tuple-element.22), channel_id=1, source_target_pairs={{0,8},{8,16},{16,24},{1,9},{9,17},{17,25},{2,10},{10,18},{18,26},{... | collective-permute-start | bytes 196616 | tf_op jit(solution)/shard_map/ppermute | solution.py:387
  11.7 1.8 %collective-permute-done.early_ref = bf16[128,256]{1,0:T(8,128)(2,1)S(1)} collective-permute-done((bf16[128,256]{1,0:T(8,128)(2,1)S(1)}, bf16[128,256]{1,0:T(8,128)(2,1)S(1)}, u32[]{:S(2)}, u32[]{:S(2)}) %collective-permute-start) | collective-permute-done | bytes 65568 | tf_op jit(solution)/shard_map/ppermute | solution.py:387
  17.0 6.9 %attend.1 = (bf16[256,128]{1,0:T(8,128)(2,1)S(1)}, bf16[256,128]{1,0:T(8,128)(2,1)S(1)}, bf16[256,128]{1,0:T(8,128)(2,1)S(1)}, bf16[256,128]{1,0:T(8,128)(2,1)S(1)}) custom-call(s32[3]{0:T(128)S(1)} %pad_add_fusion.where_ref, f32[2]{0:T(128)S(1)} %copy-done.13, bf16[1024,128]{1,0:T(8,128)(2,1)S(1)} %copy-done.12, bf16[1024,128]{1,0:T(8,128)(2,1)S(1)} %copy-done.4, ...), custom_call_target="tpu_custom_call" | custom-call | flops 4000000000 | bytes 2000000 | tf_op jit(solution)/shard_map/attend/pallas_call | solution.py:110
  24.0 2.7 %collective-permute-start.2 = (bf16[256,128]{1,0:T(8,128)(2,1)S(1)}, bf16[256,128]{1,0:T(8,128)(2,1)S(1)}, u32[]{:S(2)}, u32[]{:S(2)}) collective-permute-start(bf16[256,128]{1,0:T(8,128)(2,1)S(1)} %get-tuple-element.25), channel_id=1, source_target_pairs={{0,4},{1,5},{2,6},{3,7},{4,0},{5,1},{6,2},{7,3},{8,12},{9,13},{10,... | collective-permute-start | bytes 196616 | tf_op jit(solution)/shard_map/ppermute | solution.py:30
  27.8 3.3 %collective-permute-done.2.refs_2_ = bf16[256,128]{1,0:T(8,128)(2,1)S(1)} collective-permute-done((bf16[256,128]{1,0:T(8,128)(2,1)S(1)}, bf16[256,128]{1,0:T(8,128)(2,1)S(1)}, u32[]{:S(2)}, u32[]{:S(2)}) %collective-permute-start.2) | collective-permute-done | bytes 65568 | tf_op jit(solution)/shard_map/ppermute | solution.py:30
  31.1 24.6 %collective-permute-done.3.refs_3_ = bf16[256,128]{1,0:T(8,128)(2,1)S(1)} collective-permute-done((bf16[256,128]{1,0:T(8,128)(2,1)S(1)}, bf16[256,128]{1,0:T(8,128)(2,1)S(1)}, u32[]{:S(2)}, u32[]{:S(2)}) %collective-permute-start.3) | collective-permute-done | bytes 65568 | tf_op jit(solution)/shard_map/ppermute | solution.py:30
  55.7 3.8 %collective-permute-start.10 = (bf16[32,2176]{1,0:T(8,128)(2,1)S(1)}, bf16[32,2176]{1,0:T(8,128)(2,1)S(1)}, u32[]{:S(2)}, u32[]{:S(2)}) collective-permute-start(bf16[32,2176]{1,0:T(8,128)(2,1)S(1)} %get-tuple-element.29.refs_0_), channel_id=1, source_target_pairs={{0,6},{1,7},{2,4},{3,5},{4,2},{5,3},{6,0},{7,1},{8,14},{9,15},{10,... | collective-permute-start | bytes 417800 | tf_op jit(solution)/shard_map/ppermute | solution.py:30
  59.5 4.1 %collective-permute-done.10.refs_3_ = bf16[32,2176]{1,0:T(8,128)(2,1)S(1)} collective-permute-done((bf16[32,2176]{1,0:T(8,128)(2,1)S(1)}, bf16[32,2176]{1,0:T(8,128)(2,1)S(1)}, u32[]{:S(2)}, u32[]{:S(2)}) %collective-permute-start.10) | collective-permute-done | bytes 139296 | tf_op jit(solution)/shard_map/ppermute | solution.py:30
  63.6 1.8 %collective-permute-start.8 = (bf16[32,2176]{1,0:T(8,128)(2,1)S(1)}, bf16[32,2176]{1,0:T(8,128)(2,1)S(1)}, u32[]{:S(2)}, u32[]{:S(2)}) collective-permute-start(bf16[32,2176]{1,0:T(8,128)(2,1)S(1)} %get-tuple-element.29.refs_0_), channel_id=1, source_target_pairs={{0,2},{1,3},{2,0},{3,1},{4,6},{5,7},{6,4},{7,5},{8,10},{9,11},{10,... | collective-permute-start | bytes 417800 | tf_op jit(solution)/shard_map/ppermute | solution.py:30
  65.4 3.2 %collective-permute-done.8.refs_1_ = bf16[32,2176]{1,0:T(8,128)(2,1)S(1)} collective-permute-done((bf16[32,2176]{1,0:T(8,128)(2,1)S(1)}, bf16[32,2176]{1,0:T(8,128)(2,1)S(1)}, u32[]{:S(2)}, u32[]{:S(2)}) %collective-permute-start.8) | collective-permute-done | bytes 139296 | tf_op jit(solution)/shard_map/ppermute | solution.py:30
  68.6 2.0 %collective-permute-start.9 = (bf16[32,2176]{1,0:T(8,128)(2,1)S(1)}, bf16[32,2176]{1,0:T(8,128)(2,1)S(1)}, u32[]{:S(2)}, u32[]{:S(2)}) collective-permute-start(bf16[32,2176]{1,0:T(8,128)(2,1)S(1)} %get-tuple-element.29.refs_0_), channel_id=1, source_target_pairs={{0,4},{1,5},{2,6},{3,7},{4,0},{5,1},{6,2},{7,3},{8,12},{9,13},{10,... | collective-permute-start | bytes 417800 | tf_op jit(solution)/shard_map/ppermute | solution.py:30
  70.6 5.7 %collective-permute-done.9.refs_2_ = bf16[32,2176]{1,0:T(8,128)(2,1)S(1)} collective-permute-done((bf16[32,2176]{1,0:T(8,128)(2,1)S(1)}, bf16[32,2176]{1,0:T(8,128)(2,1)S(1)}, u32[]{:S(2)}, u32[]{:S(2)}) %collective-permute-start.9) | collective-permute-done | bytes 139296 | tf_op jit(solution)/shard_map/ppermute | solution.py:30
  78.3 2.5 %collective-permute-start.15 = (bf16[96,2048]{1,0:T(8,128)(2,1)S(1)}, bf16[96,2048]{1,0:T(8,128)(2,1)S(1)}, u32[]{:S(2)}, u32[]{:S(2)}) collective-permute-start(bf16[96,2048]{1,0:T(8,128)(2,1)S(1)} %get-tuple-element.33), channel_id=1, source_target_pairs={{0,8},{8,0},{16,24},{24,16},{1,9},{9,1},{17,25},{25,17},{2,10},{10... | collective-permute-start | bytes 1179656 | tf_op jit(solution)/shard_map/ppermute | solution.py:30
  80.8 1.7 %collective-permute-start.16 = (bf16[96,2048]{1,0:T(8,128)(2,1)S(1)}, bf16[96,2048]{1,0:T(8,128)(2,1)S(1)}, u32[]{:S(2)}, u32[]{:S(2)}) collective-permute-start(bf16[96,2048]{1,0:T(8,128)(2,1)S(1)} %get-tuple-element.34), channel_id=1, source_target_pairs={{0,16},{8,24},{16,0},{24,8},{1,17},{9,25},{17,1},{25,9},{2,18},{10... | collective-permute-start | bytes 1179656 | tf_op jit(solution)/shard_map/ppermute | solution.py:30
  83.6 6.5 %collective-permute-done.15.refs_0_ = bf16[96,2048]{1,0:T(8,128)(2,1)S(1)} collective-permute-done((bf16[96,2048]{1,0:T(8,128)(2,1)S(1)}, bf16[96,2048]{1,0:T(8,128)(2,1)S(1)}, u32[]{:S(2)}, u32[]{:S(2)}) %collective-permute-start.15) | collective-permute-done | bytes 393248 | tf_op jit(solution)/shard_map/ppermute | solution.py:30
  90.2 2.7 %collective-permute-start.11 = (bf16[96,2048]{1,0:T(8,128)(2,1)S(1)}, bf16[96,2048]{1,0:T(8,128)(2,1)S(1)}, u32[]{:S(2)}, u32[]{:S(2)}) collective-permute-start(bf16[96,2048]{1,0:T(8,128)(2,1)S(1)} %get-tuple-element.30), channel_id=1, source_target_pairs={{0,24},{8,16},{16,8},{24,0},{1,25},{9,17},{17,9},{25,1},{2,26},{10... | collective-permute-start | bytes 1179656 | tf_op jit(solution)/shard_map/ppermute | solution.py:30
  93.4 8.4 %expert.3 = (bf16[96,2048]{1,0:T(8,128)(2,1)S(1)}, bf16[96,2048]{1,0:T(8,128)(2,1)S(1)}) custom-call(bf16[96,2048]{1,0:T(8,128)(2,1)S(1)} %collective-permute-done.15.refs_0_, bf16[96,2048]{1,0:T(8,128)(2,1)S(1)} %collective-permute-done.16.refs_1_, bf16[2048,896]{1,0:T(8,128)(2,1)S(1)} %bitcast.10, bf16[2048,896]{1,0:T(8,128)(2,1)S(1)} %bitcast.13, ...), custom_call_target="tpu_custom_call" | custom-call | flops 4227858432 | bytes 22020096 | tf_op jit(solution)/shard_map/expert/pallas_call | solution.py:313
  101.8 1.5 %collective-permute-start.17 = (bf16[96,2048]{1,0:T(8,128)(2,1)S(1)}, bf16[96,2048]{1,0:T(8,128)(2,1)S(1)}, u32[]{:S(2)}, u32[]{:S(2)}) collective-permute-start(bf16[96,2048]{1,0:T(8,128)(2,1)S(1)} %get-tuple-element.35), channel_id=1, source_target_pairs={{0,8},{8,0},{16,24},{24,16},{1,9},{9,1},{17,25},{25,17},{2,10},{10... | collective-permute-start | bytes 1179656 | tf_op jit(solution)/shard_map/ppermute | solution.py:30
  103.5 8.6 %expert.2 = (bf16[96,2048]{1,0:T(8,128)(2,1)S(1)}, bf16[96,2048]{1,0:T(8,128)(2,1)S(1)}) custom-call(bf16[96,2048]{1,0:T(8,128)(2,1)S(1)} %collective-permute-done.11.refs_0_, bf16[96,2048]{1,0:T(8,128)(2,1)S(1)} %get-tuple-element.31.refs_1_, bf16[2048,896]{1,0:T(8,128)(2,1)S(1)} %bitcast.11, bf16[2048,896]{1,0:T(8,128)(2,1)S(1)} %bitcast.14, ...), custom_call_target="tpu_custom_call" | custom-call | flops 4227858432 | bytes 22020096 | tf_op jit(solution)/shard_map/expert/pallas_call | solution.py:313
  112.2 1.8 %collective-permute-start.19 = (bf16[96,2048]{1,0:T(8,128)(2,1)S(1)}, bf16[96,2048]{1,0:T(8,128)(2,1)S(1)}, u32[]{:S(2)}, u32[]{:S(2)}) collective-permute-start(bf16[96,2048]{1,0:T(8,128)(2,1)S(1)} %get-tuple-element.37), channel_id=1, source_target_pairs={{0,24},{8,16},{16,8},{24,0},{1,25},{9,17},{17,9},{25,1},{2,26},{10... | collective-permute-start | bytes 1179656 | tf_op jit(solution)/shard_map/ppermute | solution.py:30
  114.5 7.8 %collective-permute-done.19.refs_3_ = bf16[96,2048]{1,0:T(8,128)(2,1)S(1)} collective-permute-done((bf16[96,2048]{1,0:T(8,128)(2,1)S(1)}, bf16[96,2048]{1,0:T(8,128)(2,1)S(1)}, u32[]{:S(2)}, u32[]{:S(2)}) %collective-permute-start.19) | collective-permute-done | bytes 393248 | tf_op jit(solution)/shard_map/ppermute | solution.py:30
  123.5 1.6 %collective-permute-start.20 = (bf16[32,2048]{1,0:T(8,128)(2,1)S(1)}, bf16[32,2048]{1,0:T(8,128)(2,1)S(1)}, u32[]{:S(2)}, u32[]{:S(2)}) collective-permute-start(bf16[32,2048]{1,0:T(8,128)(2,1)S(1)} %get-tuple-element.39), channel_id=1, source_target_pairs={{0,2},{1,3},{2,0},{3,1},{4,6},{5,7},{6,4},{7,5},{8,10},{9,11},{10,... | collective-permute-start | bytes 393224 | tf_op jit(solution)/shard_map/ppermute | solution.py:30
  125.2 2.1 %collective-permute-start.21 = (bf16[32,2048]{1,0:T(8,128)(2,1)S(1)}, bf16[32,2048]{1,0:T(8,128)(2,1)S(1)}, u32[]{:S(2)}, u32[]{:S(2)}) collective-permute-start(bf16[32,2048]{1,0:T(8,128)(2,1)S(1)} %get-tuple-element.40), channel_id=1, source_target_pairs={{0,4},{1,5},{2,6},{3,7},{4,0},{5,1},{6,2},{7,3},{8,12},{9,13},{10,... | collective-permute-start | bytes 393224 | tf_op jit(solution)/shard_map/ppermute | solution.py:30
  129.4 6.8 %collective-permute-done.21 = bf16[32,2048]{1,0:T(8,128)(2,1)S(1)} collective-permute-done((bf16[32,2048]{1,0:T(8,128)(2,1)S(1)}, bf16[32,2048]{1,0:T(8,128)(2,1)S(1)}, u32[]{:S(2)}, u32[]{:S(2)}) %collective-permute-start.21) | collective-permute-done | bytes 131104 | tf_op jit(solution)/shard_map/ppermute | solution.py:30
  (61 shorter events, 19.7 us)
Async XLA Ops:
  0.6 92.7 %collective-permute-start.12 = (bf16[2048,896]{1,0:T(8,128)(2,1)}, bf16[2048,896]{1,0:T(8,128)(2,1)}, u32[]{:S(2)}, u32[]{:S(2)}) collective-permute-start(bf16[2048,896]{1,0:T(8,128)(2,1)} %bitcast.9), channel_id=1, source_target_pairs={{0,1},{1,0},{2,3},{3,2},{4,5},{5,4},{6,7},{7,6},{8,9},{9,8},{10,11... | collective-permute-start | bytes 11010056 | tf_op jit(solution)/shard_map/ppermute | solution.py:30
  1.2 92.1 %collective-permute-start.13 = (bf16[2048,896]{1,0:T(8,128)(2,1)}, bf16[2048,896]{1,0:T(8,128)(2,1)}, u32[]{:S(2)}, u32[]{:S(2)}) collective-permute-start(bf16[2048,896]{1,0:T(8,128)(2,1)} %bitcast.12), channel_id=1, source_target_pairs={{0,1},{1,0},{2,3},{3,2},{4,5},{5,4},{6,7},{7,6},{8,9},{9,8},{10,11... | collective-permute-start | bytes 11010056 | tf_op jit(solution)/shard_map/ppermute | solution.py:30
  1.3 92.0 %collective-permute-start.14 = (bf16[896,2048]{1,0:T(8,128)(2,1)}, bf16[896,2048]{1,0:T(8,128)(2,1)}, u32[]{:S(2)}, u32[]{:S(2)}) collective-permute-start(bf16[896,2048]{1,0:T(8,128)(2,1)} %bitcast.15), channel_id=1, source_target_pairs={{0,1},{1,0},{2,3},{3,2},{4,5},{5,4},{6,7},{7,6},{8,9},{9,8},{10,11... | collective-permute-start | bytes 11010056 | tf_op jit(solution)/shard_map/ppermute | solution.py:30
  7.1 6.4 %collective-permute-start = (bf16[128,256]{1,0:T(8,128)(2,1)S(1)}, bf16[128,256]{1,0:T(8,128)(2,1)S(1)}, u32[]{:S(2)}, u32[]{:S(2)}) collective-permute-start(bf16[128,256]{1,0:T(8,128)(2,1)S(1)} %get-tuple-element.22), channel_id=1, source_target_pairs={{0,8},{8,16},{16,24},{1,9},{9,17},{17,25},{2,10},{10,18},{18,26},{... | collective-permute-start | bytes 196616 | tf_op jit(solution)/shard_map/ppermute | solution.py:387
  17.0 76.3 %copy-start.2 = (bf16[1,896,2048]{2,1,0:T(8,128)(2,1)S(1)}, bf16[1,896,2048]{2,1,0:T(8,128)(2,1)}, u32[]{:S(2)}) copy-start(bf16[1,896,2048]{2,1,0:T(8,128)(2,1)} %param.23) | copy-start | bytes 11010052
  23.9 2.7 %collective-permute-start.1 = (bf16[256,128]{1,0:T(8,128)(2,1)S(1)}, bf16[256,128]{1,0:T(8,128)(2,1)S(1)}, u32[]{:S(2)}, u32[]{:S(2)}) collective-permute-start(bf16[256,128]{1,0:T(8,128)(2,1)S(1)} %get-tuple-element.24), channel_id=1, source_target_pairs={{0,1},{1,0},{2,3},{3,2},{4,5},{5,4},{6,7},{7,6},{8,9},{9,8},{10,11... | collective-permute-start | bytes 196616 | tf_op jit(solution)/shard_map/ppermute | solution.py:30
  24.0 7.1 %collective-permute-start.2 = (bf16[256,128]{1,0:T(8,128)(2,1)S(1)}, bf16[256,128]{1,0:T(8,128)(2,1)S(1)}, u32[]{:S(2)}, u32[]{:S(2)}) collective-permute-start(bf16[256,128]{1,0:T(8,128)(2,1)S(1)} %get-tuple-element.25), channel_id=1, source_target_pairs={{0,4},{1,5},{2,6},{3,7},{4,0},{5,1},{6,2},{7,3},{8,12},{9,13},{10,... | collective-permute-start | bytes 196616 | tf_op jit(solution)/shard_map/ppermute | solution.py:30
  26.6 49.7 %collective-permute-start.5 = (bf16[128,2048]{1,0:T(8,128)(2,1)S(1)}, bf16[128,2048]{1,0:T(8,128)(2,1)S(1)}, u32[]{:S(2)}, u32[]{:S(2)}) collective-permute-start(bf16[128,2048]{1,0:T(8,128)(2,1)S(1)} %copy-done.11), channel_id=1, source_target_pairs={{0,4},{1,5},{2,6},{3,7},{4,0},{5,1},{6,2},{7,3},{8,12},{9,13},{10,... | collective-permute-start | bytes 1572872 | tf_op jit(solution)/shard_map/ppermute | solution.py:30
  31.1 24.7 %collective-permute-start.3 = (bf16[256,128]{1,0:T(8,128)(2,1)S(1)}, bf16[256,128]{1,0:T(8,128)(2,1)S(1)}, u32[]{:S(2)}, u32[]{:S(2)}) collective-permute-start(bf16[256,128]{1,0:T(8,128)(2,1)S(1)} %get-tuple-element.26), channel_id=1, source_target_pairs={{0,5},{1,4},{2,7},{3,6},{4,1},{5,0},{6,3},{7,2},{8,13},{9,12},{10,... | collective-permute-start | bytes 196616 | tf_op jit(solution)/shard_map/ppermute | solution.py:30
  55.7 7.8 %collective-permute-start.10 = (bf16[32,2176]{1,0:T(8,128)(2,1)S(1)}, bf16[32,2176]{1,0:T(8,128)(2,1)S(1)}, u32[]{:S(2)}, u32[]{:S(2)}) collective-permute-start(bf16[32,2176]{1,0:T(8,128)(2,1)S(1)} %get-tuple-element.29.refs_0_), channel_id=1, source_target_pairs={{0,6},{1,7},{2,4},{3,5},{4,2},{5,3},{6,0},{7,1},{8,14},{9,15},{10,... | collective-permute-start | bytes 417800 | tf_op jit(solution)/shard_map/ppermute | solution.py:30
  63.6 5.1 %collective-permute-start.8 = (bf16[32,2176]{1,0:T(8,128)(2,1)S(1)}, bf16[32,2176]{1,0:T(8,128)(2,1)S(1)}, u32[]{:S(2)}, u32[]{:S(2)}) collective-permute-start(bf16[32,2176]{1,0:T(8,128)(2,1)S(1)} %get-tuple-element.29.refs_0_), channel_id=1, source_target_pairs={{0,2},{1,3},{2,0},{3,1},{4,6},{5,7},{6,4},{7,5},{8,10},{9,11},{10,... | collective-permute-start | bytes 417800 | tf_op jit(solution)/shard_map/ppermute | solution.py:30
  68.6 7.7 %collective-permute-start.9 = (bf16[32,2176]{1,0:T(8,128)(2,1)S(1)}, bf16[32,2176]{1,0:T(8,128)(2,1)S(1)}, u32[]{:S(2)}, u32[]{:S(2)}) collective-permute-start(bf16[32,2176]{1,0:T(8,128)(2,1)S(1)} %get-tuple-element.29.refs_0_), channel_id=1, source_target_pairs={{0,4},{1,5},{2,6},{3,7},{4,0},{5,1},{6,2},{7,3},{8,12},{9,13},{10,... | collective-permute-start | bytes 417800 | tf_op jit(solution)/shard_map/ppermute | solution.py:30
  76.4 1.9 %collective-permute-start.4 = (bf16[128,2048]{1,0:T(8,128)(2,1)S(1)}, bf16[128,2048]{1,0:T(8,128)(2,1)S(1)}, u32[]{:S(2)}, u32[]{:S(2)}) collective-permute-start(bf16[128,2048]{1,0:T(8,128)(2,1)S(1)} %copy-done.11), channel_id=1, source_target_pairs={{0,1},{1,0},{2,3},{3,2},{4,5},{5,4},{6,7},{7,6},{8,9},{9,8},{10,11... | collective-permute-start | bytes 1572872 | tf_op jit(solution)/shard_map/ppermute | solution.py:30
  76.4 4.4 %collective-permute-start.6 = (bf16[128,2048]{1,0:T(8,128)(2,1)S(1)}, bf16[128,2048]{1,0:T(8,128)(2,1)S(1)}, u32[]{:S(2)}, u32[]{:S(2)}) collective-permute-start(bf16[128,2048]{1,0:T(8,128)(2,1)S(1)} %collective-permute-done.5.refs_6_), channel_id=1, source_target_pairs={{0,1},{1,0},{2,3},{3,2},{4,5},{5,4},{6,7},{7,6},{8,9},{9,8},{10,11... | collective-permute-start | bytes 1572872 | tf_op jit(solution)/shard_map/ppermute | solution.py:30
  78.3 11.9 %collective-permute-start.15 = (bf16[96,2048]{1,0:T(8,128)(2,1)S(1)}, bf16[96,2048]{1,0:T(8,128)(2,1)S(1)}, u32[]{:S(2)}, u32[]{:S(2)}) collective-permute-start(bf16[96,2048]{1,0:T(8,128)(2,1)S(1)} %get-tuple-element.33), channel_id=1, source_target_pairs={{0,8},{8,0},{16,24},{24,16},{1,9},{9,1},{17,25},{25,17},{2,10},{10... | collective-permute-start | bytes 1179656 | tf_op jit(solution)/shard_map/ppermute | solution.py:30
  80.8 12.1 %collective-permute-start.16 = (bf16[96,2048]{1,0:T(8,128)(2,1)S(1)}, bf16[96,2048]{1,0:T(8,128)(2,1)S(1)}, u32[]{:S(2)}, u32[]{:S(2)}) collective-permute-start(bf16[96,2048]{1,0:T(8,128)(2,1)S(1)} %get-tuple-element.34), channel_id=1, source_target_pairs={{0,16},{8,24},{16,0},{24,8},{1,17},{9,25},{17,1},{25,9},{2,18},{10... | collective-permute-start | bytes 1179656 | tf_op jit(solution)/shard_map/ppermute | solution.py:30
  90.2 13.4 %collective-permute-start.11 = (bf16[96,2048]{1,0:T(8,128)(2,1)S(1)}, bf16[96,2048]{1,0:T(8,128)(2,1)S(1)}, u32[]{:S(2)}, u32[]{:S(2)}) collective-permute-start(bf16[96,2048]{1,0:T(8,128)(2,1)S(1)} %get-tuple-element.30), channel_id=1, source_target_pairs={{0,24},{8,16},{16,8},{24,0},{1,25},{9,17},{17,9},{25,1},{2,26},{10... | collective-permute-start | bytes 1179656 | tf_op jit(solution)/shard_map/ppermute | solution.py:30
  92.9 35.6 %collective-permute-start.7 = (bf16[128,2048]{1,0:T(8,128)(2,1)S(1)}, bf16[128,2048]{1,0:T(8,128)(2,1)S(1)}, u32[]{:S(2)}, u32[]{:S(2)}) collective-permute-start(bf16[128,2048]{1,0:T(8,128)(2,1)S(1)} %get-tuple-element.28), channel_id=1, source_target_pairs={{0,2},{1,3},{2,0},{3,1},{4,6},{5,7},{6,4},{7,5},{8,10},{9,11},{10,... | collective-permute-start | bytes 1572872 | tf_op jit(solution)/shard_map/ppermute | solution.py:30
  101.8 12.7 %collective-permute-start.17 = (bf16[96,2048]{1,0:T(8,128)(2,1)S(1)}, bf16[96,2048]{1,0:T(8,128)(2,1)S(1)}, u32[]{:S(2)}, u32[]{:S(2)}) collective-permute-start(bf16[96,2048]{1,0:T(8,128)(2,1)S(1)} %get-tuple-element.35), channel_id=1, source_target_pairs={{0,8},{8,0},{16,24},{24,16},{1,9},{9,1},{17,25},{25,17},{2,10},{10... | collective-permute-start | bytes 1179656 | tf_op jit(solution)/shard_map/ppermute | solution.py:30
  103.3 11.2 %collective-permute-start.18 = (bf16[96,2048]{1,0:T(8,128)(2,1)S(1)}, bf16[96,2048]{1,0:T(8,128)(2,1)S(1)}, u32[]{:S(2)}, u32[]{:S(2)}) collective-permute-start(bf16[96,2048]{1,0:T(8,128)(2,1)S(1)} %get-tuple-element.36), channel_id=1, source_target_pairs={{0,16},{8,24},{16,0},{24,8},{1,17},{9,25},{17,1},{25,9},{2,18},{10... | collective-permute-start | bytes 1179656 | tf_op jit(solution)/shard_map/ppermute | solution.py:30
  112.2 10.1 %collective-permute-start.19 = (bf16[96,2048]{1,0:T(8,128)(2,1)S(1)}, bf16[96,2048]{1,0:T(8,128)(2,1)S(1)}, u32[]{:S(2)}, u32[]{:S(2)}) collective-permute-start(bf16[96,2048]{1,0:T(8,128)(2,1)S(1)} %get-tuple-element.37), channel_id=1, source_target_pairs={{0,24},{8,16},{16,8},{24,0},{1,25},{9,17},{17,9},{25,1},{2,26},{10... | collective-permute-start | bytes 1179656 | tf_op jit(solution)/shard_map/ppermute | solution.py:30
  123.5 5.8 %collective-permute-start.20 = (bf16[32,2048]{1,0:T(8,128)(2,1)S(1)}, bf16[32,2048]{1,0:T(8,128)(2,1)S(1)}, u32[]{:S(2)}, u32[]{:S(2)}) collective-permute-start(bf16[32,2048]{1,0:T(8,128)(2,1)S(1)} %get-tuple-element.39), channel_id=1, source_target_pairs={{0,2},{1,3},{2,0},{3,1},{4,6},{5,7},{6,4},{7,5},{8,10},{9,11},{10,... | collective-permute-start | bytes 393224 | tf_op jit(solution)/shard_map/ppermute | solution.py:30
  125.2 11.0 %collective-permute-start.21 = (bf16[32,2048]{1,0:T(8,128)(2,1)S(1)}, bf16[32,2048]{1,0:T(8,128)(2,1)S(1)}, u32[]{:S(2)}, u32[]{:S(2)}) collective-permute-start(bf16[32,2048]{1,0:T(8,128)(2,1)S(1)} %get-tuple-element.40), channel_id=1, source_target_pairs={{0,4},{1,5},{2,6},{3,7},{4,0},{5,1},{6,2},{7,3},{8,12},{9,13},{10,... | collective-permute-start | bytes 393224 | tf_op jit(solution)/shard_map/ppermute | solution.py:30
  127.3 8.9 %collective-permute-start.22 = (bf16[32,2048]{1,0:T(8,128)(2,1)S(1)}, bf16[32,2048]{1,0:T(8,128)(2,1)S(1)}, u32[]{:S(2)}, u32[]{:S(2)}) collective-permute-start(bf16[32,2048]{1,0:T(8,128)(2,1)S(1)} %get-tuple-element.41), channel_id=1, source_target_pairs={{0,6},{1,7},{2,4},{3,5},{4,2},{5,3},{6,0},{7,1},{8,14},{9,15},{10,... | collective-permute-start | bytes 393224 | tf_op jit(solution)/shard_map/ppermute | solution.py:30
  (13 other events, 39.9 us)

commit v2 on v1

--- a/solution.py
+++ b/solution.py
@@ -41,6 +41,10 @@
     return copies
 
 
+def far_away(value):
+    return pltpu.with_memory_space_constraint(value, pltpu.HBM)
+
+
 def cost(flops, moved):
     return pl.CostEstimate(flops=int(flops), bytes_accessed=int(moved), transcendentals=0)
 
@@ -51,15 +55,15 @@
 
 def relative(i, groups_z):
     far, core, k = i // (2 * groups_z), (i // groups_z) % 2, i % groups_z
-    return far * (2 * groups_z) + 2 * k + core
+    return 2 * CORES * k + CORES * far + core
 
 
 def attend_kernel(where_ref, sink_ref, q_hbm, k_hbm, v_hbm, early_ref, *refs):
-    out_refs, (q_ref, k_ref, v_ref, sems) = refs[:4], refs[4:]
-    for copy in fetch((q_hbm, k_hbm, v_hbm), (q_ref, k_ref, v_ref), sems):
-        copy.wait()
+    out_refs, (q_ref, kv_ref, k_ext, v_ext, sems) = refs[:3], refs[3:]
+    copies = fetch((q_hbm, k_hbm, v_hbm), (q_ref, kv_ref.at[0], kv_ref.at[1]), sems)
     blocks = q_ref.shape[0] // WINDOW
-    heads_here = q_ref.shape[1] // HEAD_DIM
+    cols = q_ref.shape[1]
+    heads_here = cols // HEAD_DIM
     groups_z = blocks // 4
     key_head = where_ref[1]
     width = KV_HEADS * HEAD_DIM
@@ -71,34 +75,45 @@
             picked = jnp.where(key_head == h, parts[h], picked)
         return picked
 
-    row = lax.broadcasted_iota(jnp.int32, (WINDOW, WINDOW), 0)
-    col = lax.broadcasted_iota(jnp.int32, (WINDOW, WINDOW), 1)
-    cur_ok = col <= row
+    k_ext[...] = jnp.zeros_like(k_ext)
+    v_ext[:, :, :cols] = jnp.zeros((heads_here, v_ext.shape[1], cols), BF)
+    v_ext[:, :, cols:] = jnp.ones((heads_here, v_ext.shape[1], cols), BF)
+    early_k, early_v = own(early_ref[:, :width]), own(early_ref[:, width:])
+    for h in range(heads_here):
+        place = slice(h * HEAD_DIM, (h + 1) * HEAD_DIM)
+        k_ext[h, :WINDOW, place] = early_k
+        v_ext[h, :WINDOW, place] = early_v
+    for copy in copies:
+        copy.wait()
+    own_k, own_v = own(kv_ref[0]), own(kv_ref[1])
+    for h in range(heads_here):
+        place = slice(h * HEAD_DIM, (h + 1) * HEAD_DIM)
+        k_ext[h, WINDOW:, place] = own_k
+        v_ext[h, WINDOW:, place] = own_v
+
+    row = lax.broadcasted_iota(jnp.int32, (WINDOW, 2 * WINDOW), 0)
+    col = lax.broadcasted_iota(jnp.int32, (WINDOW, 2 * WINDOW), 1)
+    near = jnp.logical_and(col > row, col <= row + WINDOW)
     for i in range(blocks):
         block = where_ref[0] ^ relative(i, groups_z)
-        first = block == 0
-        no_past = jnp.logical_and(first, where_ref[2] == 0)
-        here = pl.ds(pl.multiple_of(block * WINDOW, WINDOW), WINDOW)
-        past = pl.ds(pl.multiple_of(jnp.maximum(block - 1, 0) * WINDOW, WINDOW), WINDOW)
-        k_cur, v_cur = own(k_ref[here, :]), own(v_ref[here, :])
-        k_past = own(jnp.where(first, early_ref[:, :width], k_ref[past, :]))
-        v_past = own(jnp.where(first, early_ref[:, width:], v_ref[past, :]))
-        past_ok = jnp.logical_and(col > row, jnp.logical_not(no_past))
-        out_ref, place = out_refs[i // groups_z], (i % groups_z) * WINDOW
+        no_past = jnp.logical_and(block == 0, where_ref[2] == 0)
+        allowed = jnp.logical_and(near, col >= jnp.where(no_past, WINDOW, 0))
+        start = pl.multiple_of(block * WINDOW, WINDOW)
+        q = q_ref[pl.ds(start, WINDOW), :] * HEAD_DIM ** (-0.5)
+        mixed = None
         for h in range(heads_here):
-            cols = slice(h * HEAD_DIM, (h + 1) * HEAD_DIM)
-            q = q_ref[here, cols]
             sink = sink_ref[h]
-            s_past = jnp.where(past_ok, nt(q, k_past) * HEAD_DIM ** (-0.5), big_negative)
-            s_cur = jnp.where(cur_ok, nt(q, k_cur) * HEAD_DIM ** (-0.5), big_negative)
-            top = jnp.maximum(jnp.max(jnp.maximum(s_past, s_cur), -1, keepdims=True), sink)
-            e_past = jnp.where(past_ok, jnp.exp(s_past - top), 0.0)
-            e_cur = jnp.where(cur_ok, jnp.exp(s_cur - top), 0.0)
-            total = jnp.sum(e_past + e_cur, -1, keepdims=True) + jnp.exp(sink - top)
-            scale = 1.0 / total
-            mixed = jnp.dot((e_past * scale).astype(BF), v_past, preferred_element_type=F32)
-            mixed += jnp.dot((e_cur * scale).astype(BF), v_cur, preferred_element_type=F32)
-            out_ref[place : place + WINDOW, cols] = mixed.astype(BF)
+            window = pl.ds(start, 2 * WINDOW)
+            scores = jnp.where(allowed, nt(q, k_ext[h, window, :]), big_negative)
+            top = jnp.maximum(jnp.max(scores, -1, keepdims=True), sink)
+            powers = jnp.exp(scores - top).astype(BF)
+            both = jnp.dot(powers, v_ext[h, window, :], preferred_element_type=F32)
+            part = both[:, :cols] / (both[:, cols:] + jnp.exp(sink - top))
+            mixed = part if mixed is None else mixed + part
+        group, place = i // groups_z, i % groups_z
+        if group >= 2:
+            place += (group - 2) * groups_z
+        out_refs[min(group, 2)][place * WINDOW : (place + 1) * WINDOW, :] = mixed.astype(BF)
 
 
 def attend(queries, key_rows, value_rows, sink_logits, earlier):
@@ -110,25 +125,32 @@
     return pl.pallas_call(
         attend_kernel,
         in_specs=[SMEM, SMEM] + [HBM] * 3 + [VMEM],
-        out_specs=[VMEM] * 4,
-        out_shape=[jax.ShapeDtypeStruct((total // 4, cols), BF)] * 4,
-        scratch_shapes=[pltpu.VMEM(a.shape, BF) for a in (queries, key_rows, value_rows)]
-        + [pltpu.SemaphoreType.DMA((3,))],
+        out_specs=[VMEM] * 3,
+        out_shape=[jax.ShapeDtypeStruct((total // n, cols), BF) for n in (4, 4, 2)],
+        scratch_shapes=[
+            pltpu.VMEM(queries.shape, BF),
+            pltpu.VMEM((2,) + key_rows.shape, BF),
+            pltpu.VMEM((cols // HEAD_DIM, total + WINDOW, cols), BF),
+            pltpu.VMEM((cols // HEAD_DIM, total + WINDOW, 2 * cols), BF),
+            pltpu.SemaphoreType.DMA((3,)),
+        ],
         cost_estimate=cost(4e9, 2e6),
         compiler_params=small(8),
         name="attend",
-    )(place, sink_logits, queries, key_rows, value_rows, earlier)
-
-
-def project_kernel(count, *refs):
-    parts, mats, outs = refs[:count], refs[count : 2 * count], refs[2 * count :]
+    )(place, sink_logits, *map(far_away, (queries, key_rows, value_rows)), earlier)
+
+
+def project_kernel(*refs):
+    parts, mats, outs = refs[:4], refs[4:8], refs[8:]
     rows = outs[0].shape[0]
+    here = parts[0].shape[0]
     width = mats[0].shape[1]
     tile = min(512, width)
     for n in range(0, width, tile):
         total = None
-        for part, mat in zip(parts, mats):
-            term = jnp.dot(part[...], mat[:, n : n + tile], preferred_element_type=F32)
+        for i, (part, mat) in enumerate(zip(parts, mats)):
+            left = part[here:, :] if i == 3 else part[:here, :]
+            term = jnp.dot(left, mat[:, n : n + tile], preferred_element_type=F32)
             total = term if total is None else total + term
         for i, out in enumerate(outs):
             out[:, n : n + tile] = total[i * rows : (i + 1) * rows].astype(out.dtype)
@@ -140,8 +162,8 @@
     groups = rows // WINDOW
     out = [jax.ShapeDtypeStruct((WINDOW, width), F32 if i == 0 else BF) for i in range(groups)]
     return pl.pallas_call(
-        functools.partial(project_kernel, len(parts)),
-        in_specs=[VMEM] * (2 * len(parts)),
+        project_kernel,
+        in_specs=[VMEM] * 8,
         out_specs=[VMEM] * groups,
         out_shape=out,
         cost_estimate=cost(2e9, 4e6),
@@ -192,7 +214,7 @@
         cost_estimate=cost(1e7, 3e5),
         compiler_params=small(8),
         name="normed",
-    )(*args)
+    )(*map(far_away, args))
 
 
 def slots_of(experts, capacity, blocks, width):
@@ -274,57 +296,72 @@
     )(ep, *blocks)
 
 
-def expert_kernel(count, *refs):
-    rows_refs = refs[:count]
-    own_mats, other_mats = refs[count : count + 3], refs[count + 3 : count + 6]
-    outs = refs[count + 6 : 2 * count + 6]
-    all_rows, hidden, sems = refs[2 * count + 6 : 2 * count + 9]
-    held = refs[2 * count + 9 :]
-    copies = fetch(other_mats, held, sems)
-    gates, ups, downs = zip(own_mats, held)
+def expert_kernel(count, fetching, *refs):
+    rows_refs, mats, refs = refs[:count], (refs[count : count + 3], refs[count + 3 : count + 6]), refs[count + 6 :]
+    outs, refs = refs[:count], refs[count:]
+    copies = [None] * 3
+    if fetching:
+        held, refs = refs[:3], refs[3:]
+        copies = fetch(mats[1], held, refs[3])
+        mats = mats[0], held
+    all_rows, hidden, total = refs[:3]
     slots, width = rows_refs[0].shape
-    units = gates[0].shape[1]
+    units = mats[0][0].shape[1]
     for i in range(count):
         all_rows[i * slots : (i + 1) * slots, :] = rows_refs[i][...]
     tile = 256
-    for j in range(2):
-        if j == 1:
+    for j, (gate, up, down) in enumerate(mats):
+        if fetching and j == 1:
             copies[0].wait()
             copies[1].wait()
         for n in range(0, units, tile):
             cols = slice(n, min(n + tile, units))
-            g = jnp.dot(all_rows[...], gates[j][:, cols], preferred_element_type=F32)
-            u = jnp.dot(all_rows[...], ups[j][:, cols], preferred_element_type=F32)
+            g = jnp.dot(all_rows[...], gate[:, cols], preferred_element_type=F32)
+            u = jnp.dot(all_rows[...], up[:, cols], preferred_element_type=F32)
             hidden[j, :, cols] = (g / (1.0 + jnp.exp(-g)) * u).astype(BF)
-    copies[2].wait()
+        if fetching and j == 0:
+            for n in range(0, width, tile):
+                cols = slice(n, n + tile)
+                total[:, cols] = jnp.dot(hidden[0], down[:, cols], preferred_element_type=F32)
+    if fetching:
+        copies[2].wait()
     for n in range(0, width, tile):
         cols = slice(n, n + tile)
-        total = jnp.dot(hidden[0], downs[0][:, cols], preferred_element_type=F32)
-        total += jnp.dot(hidden[1], downs[1][:, cols], preferred_element_type=F32)
+        if fetching:
+            term = total[:, cols]
+        else:
+            term = jnp.dot(hidden[0], mats[0][2][:, cols], preferred_element_type=F32)
+        term += jnp.dot(hidden[1], mats[1][2][:, cols], preferred_element_type=F32)
         for i in range(count):
-            outs[i][:, cols] = total[i * slots : (i + 1) * slots].astype(BF)
-
-
-def expert(row_sets, own_mats, other_mats):
+            outs[i][:, cols] = term[i * slots : (i + 1) * slots].astype(BF)
+
+
+def expert(row_sets, own_mats, other_mats, fetching):
     count = len(row_sets)
     slots, width = row_sets[0].shape
     units = own_mats[0].shape[1]
     total = count * slots
-    return pl.pallas_call(
-        functools.partial(expert_kernel, count),
-        in_specs=[VMEM] * (count + 3) + [HBM] * 3,
-        out_specs=[VMEM] * count,
-        out_shape=[jax.ShapeDtypeStruct((slots, width), BF)] * count,
-        scratch_shapes=[
-            pltpu.VMEM((total, width), BF),
-            pltpu.VMEM((2, total, units), BF),
-            pltpu.SemaphoreType.DMA((3,)),
-        ]
-        + [pltpu.VMEM(m.shape, BF) for m in other_mats],
+    out = [jax.ShapeDtypeStruct((slots, width), BF)] * count
+    scratch = [
+        pltpu.VMEM((total, width), BF),
+        pltpu.VMEM((2, total, units), BF),
+        pltpu.VMEM((total, width), F32),
+    ]
+    if fetching:
+        out += [jax.ShapeDtypeStruct(m.shape, BF) for m in other_mats]
+        scratch.append(pltpu.SemaphoreType.DMA((3,)))
+        other_mats = list(map(far_away, other_mats))
+    result = pl.pallas_call(
+        functools.partial(expert_kernel, count, fetching),
+        in_specs=[VMEM] * (count + 3) + [HBM if fetching else VMEM] * 3,
+        out_specs=[VMEM] * len(out),
+        out_shape=out,
+        scratch_shapes=scratch,
         cost_estimate=cost(12 * total * width * units, 12 * width * units),
-        compiler_params=small(22),
+        compiler_params=small(16),
         name="expert",
     )(*row_sets, *own_mats, *other_mats)
+    return result[:count], result[count:] if fetching else other_mats
 
 
 def combine_kernel(experts, maps_ref, *refs):
@@ -342,11 +379,11 @@
             out[:, cols] = total[i * rows : (i + 1) * rows].astype(out.dtype)
 
 
-def combine(maps, results, lines):
+def combine(maps, results, lines, kept):
     experts = len(results)
     width = results[0].shape[1]
     rows = maps.shape[1] // lines
-    out = [jax.ShapeDtypeStruct((rows, width), F32 if i == 0 else BF) for i in range(lines)]
+    out = [jax.ShapeDtypeStruct((rows, width), F32 if i == 0 and kept else BF) for i in range(lines)]
     return pl.pallas_call(
         functools.partial(combine_kernel, experts),
         in_specs=[VMEM] * (1 + experts),
@@ -373,44 +410,37 @@
     down_weight,
 ):
     tp, ep = lax.axis_size("tp"), lax.axis_size("ep")
-    lines, far = tp // CORES, tp // 2
+    lines, far = tp // CORES, CORES
     experts_all = gate_weight.shape[0] * ep
     capacity = 3 * moe_rows.shape[0] * TOP // (2 * experts_all)
-
-    own_mats = (gate_weight[0], up_weight[0], down_weight[0])
-    other_mats = [swapped(m, "tp", 1) for m in own_mats]
 
     own, last = normed_rows(
         moe_rows, moe_gain, routes, route_weight, experts_all, key_rows, value_rows
     )
     blocks = [own] + [swapped(own, "tp", CORES * k) for k in range(1, lines)]
     earlier = lax.ppermute(last, "ep", [(i, i + 1) for i in range(ep - 1)])
-
-    picked = pick(blocks, experts_all, capacity)
-    arrived = [picked[0]] + [swapped(picked[k], "ep", k) for k in range(1, ep)]
-    maps = weight_maps(blocks, experts_all, capacity)
+    own_mats = (gate_weight[0], up_weight[0], down_weight[0])
+    other_mats = [swapped(m, "tp", 1) for m in own_mats]
 
     pieces = attend(queries, key_rows, value_rows, sink_logits, earlier)
-    parts = [pieces[0]] + [
-        swapped(pieces[i], "tp", mask)
-        for i, mask in ((1, 1), (2, far), (3, far + 1))
-    ]
+    far_heads = swapped(pieces[2], "tp", far)
+    parts = [pieces[0], swapped(pieces[1], "tp", 1), far_heads, swapped(far_heads, "tp", 1)]
     far_weight = swapped(out_weight, "tp", far)
     mats = [out_weight, swapped(out_weight, "tp", 1), far_weight, swapped(far_weight, "tp", 1)]
     shares = project(parts, mats)
     mixer = shares[0]
-    for k in range(1, far // CORES):
-        mixer += swapped(shares[k], "tp", CORES * k).astype(F32)
-
-    order = list(range(1, ep)) + [0]
-    results = [None] * ep
-    for group in (order[: ep // 2], order[ep // 2 :]):
-        done = expert([arrived[k] for k in group], own_mats, other_mats)
-        for k, value in zip(group, done):
-            results[k] = value
-    returned = [results[0]] + [swapped(results[k], "ep", k) for k in range(1, ep)]
-
-    sums = combine(maps, returned, lines)
+    for k in range(1, lines // 2):
+        mixer += swapped(shares[k], "tp", 2 * CORES * k).astype(F32)
+
+    middle = lines // 2
+    sums = []
+    for name, group in (("N", blocks[:middle]), ("F", blocks[middle:])):
+        picked = pick(group, experts_all, capacity)
+        maps = weight_maps(group, experts_all, capacity)
+        arrived = [picked[0]] + [swapped(picked[k], "ep", k) for k in range(1, ep)]
+        done, other_mats = expert(arrived, own_mats, other_mats, name == "N")
+        returned = [done[0]] + [swapped(done[k], "ep", k) for k in range(1, ep)]
+        sums += combine(maps, returned, len(group), name == "N")
     moe = sums[0]
     for k in range(1, lines):
         moe += swapped(sums[k], "tp", CORES * k).astype(F32)

time: 137 us -> 113 us (0.82)
  waiting for transfers between devices: 64.4 us -> 47.3 us
  local copies, waits for them, and re-layouts: 8.37 us -> 0.67 us
  starting transfers between devices: 33.5 us -> 40.6 us
  Pallas kernels: 28.1 us -> 21.9 us
    ppermute x22 -> x28, waiting for transfers between devices: 62.6 us -> 45.5 us  [swapped(): return lax.ppermute(value, axis, [(i, i ^ mask) for i in range(count)])]
    ppermute x22 -> x28, starting transfers between devices: 29 us -> 37.2 us  [swapped(): return lax.ppermute(value, axis, [(i, i ^ mask) for i in range(count)])]
    unnamed x28 -> x10, local copies, waits for them, and re-layouts: 8.37 us -> 0.67 us
    pallas_call x3, Pallas kernels: 18.2 us -> 13.9 us  [the longest x2 12.7 us: expert(): pl.pallas_call(functools.partial(expert_kernel, count, fetching), in_spec...]
    pallas_call x1, Pallas kernels: 6.89 us -> 3.48 us  [attend(): pl.pallas_call(attend_kernel, in_specs=[SMEM, SMEM] + [HBM] * 3 + [VMEM],...]
  transfers between devices with their start and end apart: 23 -> 29, of which waited for: 10 -> 11; matrix products, arithmetic and copies ran while one was open for 1% -> 1% of each run, Pallas kernels for 21% -> 19%
where the time goes in v2:
time: 113 us
  waiting for transfers between devices  47.3 us (42%)
  starting transfers between devices  40.6 us (36%)
  Pallas kernels  21.9 us (19%)
  other arithmetic  1.69 us (1%)
    ppermute x28, waiting for transfers between devices, swapped(): return lax.ppermute(value, axis, [(i, i ^ mask) for i in range(count)])  45.5 us
    ppermute x28, starting transfers between devices, swapped(): return lax.ppermute(value, axis, [(i, i ^ mask) for i in range(count)])  37.2 us
    pallas_call x2, Pallas kernels, expert(): pl.pallas_call(functools.partial(expert_kernel, count, fetching), in_spec...  12.7 us
    pallas_call x1, Pallas kernels, attend(): pl.pallas_call(attend_kernel, in_specs=[SMEM, SMEM] + [HBM] * 3 + [VMEM],...  3.48 us
    ppermute x1, starting transfers between devices, body(): earlier = lax.ppermute(last, 'ep', [(i, i + 1) for i in range(ep - 1)])  3.39 us
  transfers between devices with their start and end apart: 29, of which 11 were waited for; matrix products, arithmetic and copies ran while one was open for 1% of the time, Pallas kernels for 19%

profile of v2, /device:TPU:0, one launch (start us, length us, event | category | flops | bytes accessed | tf_op | source)
XLA Modules:
  0.0 113.0 jit_solution(12379059444879837534)
XLA Ops:
  2.9 2.7 %collective-permute-start.8 = (bf16[32,2176]{1,0:T(8,128)(2,1)S(1)}, bf16[32,2176]{1,0:T(8,128)(2,1)S(1)}, u32[]{:S(2)}, u32[]{:S(2)}) collective-permute-start(bf16[32,2176]{1,0:T(8,128)(2,1)S(1)} %get-tuple-element.38.refs_0_), channel_id=1, source_target_pairs={{0,2},{1,3},{2,0},{3,1},{4,6},{5,7},{6,4},{7,5},{8,10},{9,11},{10,... | collective-permute-start | bytes 417800 | tf_op jit(solution)/shard_map/ppermute | solution.py:30
  5.6 3.4 %collective-permute-start = (bf16[128,256]{1,0:T(8,128)(2,1)S(1)}, bf16[128,256]{1,0:T(8,128)(2,1)S(1)}, u32[]{:S(2)}, u32[]{:S(2)}) collective-permute-start(bf16[128,256]{1,0:T(8,128)(2,1)S(1)} %get-tuple-element.32), channel_id=1, source_target_pairs={{0,8},{8,16},{16,24},{1,9},{9,17},{17,25},{2,10},{10,18},{18,26},{... | collective-permute-start | bytes 196616 | tf_op jit(solution)/shard_map/ppermute | solution.py:421
  9.1 1.8 %collective-permute-done.early_ref = bf16[128,256]{1,0:T(8,128)(2,1)S(1)} collective-permute-done((bf16[128,256]{1,0:T(8,128)(2,1)S(1)}, bf16[128,256]{1,0:T(8,128)(2,1)S(1)}, u32[]{:S(2)}, u32[]{:S(2)}) %collective-permute-start) | collective-permute-done | bytes 65568 | tf_op jit(solution)/shard_map/ppermute | solution.py:421
  11.5 3.5 %attend.1 = (bf16[256,128]{1,0:T(8,128)(2,1)S(1)}, bf16[256,128]{1,0:T(8,128)(2,1)S(1)}, bf16[512,128]{1,0:T(8,128)(2,1)S(1)}) custom-call(s32[3]{0:T(128)S(1)} %pad_add_fusion.where_ref, f32[2]{0:T(128)S(1)} %copy-done.4, bf16[1024,128]{1,0:T(8,128)(2,1)} %q_hbm.1, bf16[1024,128]{1,0:T(8,128)(2,1)} %k_hbm.1, bf16[1024,128]{1,0:T(8,128)(2,1)} %v_hbm.1, ...), custom_call_target="tpu_custom_call" | custom-call | flops 4000000000 | bytes 2000000 | tf_op jit(solution)/shard_map/attend/pallas_call | solution.py:125
  15.1 3.0 %collective-permute-done.1.refs_1_ = bf16[256,128]{1,0:T(8,128)(2,1)S(1)} collective-permute-done((bf16[256,128]{1,0:T(8,128)(2,1)S(1)}, bf16[256,128]{1,0:T(8,128)(2,1)S(1)}, u32[]{:S(2)}, u32[]{:S(2)}) %collective-permute-start.1) | collective-permute-done | bytes 65568 | tf_op jit(solution)/shard_map/ppermute | solution.py:30
  18.1 3.9 %collective-permute-start.19 = (bf16[32,2176]{1,0:T(8,128)(2,1)S(1)}, bf16[32,2176]{1,0:T(8,128)(2,1)S(1)}, u32[]{:S(2)}, u32[]{:S(2)}) collective-permute-start(bf16[32,2176]{1,0:T(8,128)(2,1)S(1)} %get-tuple-element.38.refs_0_), channel_id=1, source_target_pairs={{0,4},{1,5},{2,6},{3,7},{4,0},{5,1},{6,2},{7,3},{8,12},{9,13},{10,... | collective-permute-start | bytes 417800 | tf_op jit(solution)/shard_map/ppermute | solution.py:30
  23.4 9.1 %collective-permute-done.19.refs_0_ = bf16[32,2176]{1,0:T(8,128)(2,1)S(1)} collective-permute-done((bf16[32,2176]{1,0:T(8,128)(2,1)S(1)}, bf16[32,2176]{1,0:T(8,128)(2,1)S(1)}, u32[]{:S(2)}, u32[]{:S(2)}) %collective-permute-start.19) | collective-permute-done | bytes 139296 | tf_op jit(solution)/shard_map/ppermute | solution.py:30
  32.8 2.9 %collective-permute-start.2 = (bf16[512,128]{1,0:T(8,128)(2,1)S(1)}, bf16[512,128]{1,0:T(8,128)(2,1)S(1)}, u32[]{:S(2)}, u32[]{:S(2)}) collective-permute-start(bf16[512,128]{1,0:T(8,128)(2,1)S(1)} %get-tuple-element.35), channel_id=1, source_target_pairs={{0,2},{1,3},{2,0},{3,1},{4,6},{5,7},{6,4},{7,5},{8,10},{9,11},{10,... | collective-permute-start | bytes 393224 | tf_op jit(solution)/shard_map/ppermute | solution.py:30
  35.7 12.5 %collective-permute-done.2.refs_2_ = bf16[512,128]{1,0:T(8,128)(2,1)S(1)} collective-permute-done((bf16[512,128]{1,0:T(8,128)(2,1)S(1)}, bf16[512,128]{1,0:T(8,128)(2,1)S(1)}, u32[]{:S(2)}, u32[]{:S(2)}) %collective-permute-start.2) | collective-permute-done | bytes 131104 | tf_op jit(solution)/shard_map/ppermute | solution.py:30
  50.8 5.7 %collective-permute-done.10.refs_2_ = bf16[48,2048]{1,0:T(8,128)(2,1)S(1)} collective-permute-done((bf16[48,2048]{1,0:T(8,128)(2,1)S(1)}, bf16[48,2048]{1,0:T(8,128)(2,1)S(1)}, u32[]{:S(2)}, u32[]{:S(2)}) %collective-permute-start.10) | collective-permute-done | bytes 196640 | tf_op jit(solution)/shard_map/ppermute | solution.py:30
  57.0 1.4 %collective-permute-done.4.refs_5_ = bf16[128,2048]{1,0:T(8,128)(2,1)S(1)} collective-permute-done((bf16[128,2048]{1,0:T(8,128)(2,1)S(1)}, bf16[128,2048]{1,0:T(8,128)(2,1)S(1)}, u32[]{:S(2)}, u32[]{:S(2)}) %collective-permute-start.4) | collective-permute-done | bytes 524320 | tf_op jit(solution)/shard_map/ppermute | solution.py:30
  58.4 2.2 %collective-permute-start.11 = (bf16[48,2048]{1,0:T(8,128)(2,1)S(1)}, bf16[48,2048]{1,0:T(8,128)(2,1)S(1)}, u32[]{:S(2)}, u32[]{:S(2)}) collective-permute-start(bf16[48,2048]{1,0:T(8,128)(2,1)S(1)} %get-tuple-element.42), channel_id=1, source_target_pairs={{0,24},{8,16},{16,8},{24,0},{1,25},{9,17},{17,9},{25,1},{2,26},{10... | collective-permute-start | bytes 589832 | tf_op jit(solution)/shard_map/ppermute | solution.py:30
  63.0 4.1 %collective-permute-done.11.refs_3_ = bf16[48,2048]{1,0:T(8,128)(2,1)S(1)} collective-permute-done((bf16[48,2048]{1,0:T(8,128)(2,1)S(1)}, bf16[48,2048]{1,0:T(8,128)(2,1)S(1)}, u32[]{:S(2)}, u32[]{:S(2)}) %collective-permute-start.11) | collective-permute-done | bytes 196640 | tf_op jit(solution)/shard_map/ppermute | solution.py:30
  68.3 2.8 %collective-permute-done.9.refs_1_ = bf16[48,2048]{1,0:T(8,128)(2,1)S(1)} collective-permute-done((bf16[48,2048]{1,0:T(8,128)(2,1)S(1)}, bf16[48,2048]{1,0:T(8,128)(2,1)S(1)}, u32[]{:S(2)}, u32[]{:S(2)}) %collective-permute-start.9) | collective-permute-done | bytes 196640 | tf_op jit(solution)/shard_map/ppermute | solution.py:30
  71.8 2.2 %collective-permute-start.23 = (bf16[48,2048]{1,0:T(8,128)(2,1)S(1)}, bf16[48,2048]{1,0:T(8,128)(2,1)S(1)}, u32[]{:S(2)}, u32[]{:S(2)}) collective-permute-start(bf16[48,2048]{1,0:T(8,128)(2,1)S(1)} %get-tuple-element.52), channel_id=1, source_target_pairs={{0,24},{8,16},{16,8},{24,0},{1,25},{9,17},{17,9},{25,1},{2,26},{10... | collective-permute-start | bytes 589832 | tf_op jit(solution)/shard_map/ppermute | solution.py:30
  74.0 3.1 %collective-permute-start.7 = (bf16[128,2048]{1,0:T(8,128)(2,1)S(1)}, bf16[128,2048]{1,0:T(8,128)(2,1)S(1)}, u32[]{:S(2)}, u32[]{:S(2)}) collective-permute-start(bf16[128,2048]{1,0:T(8,128)(2,1)S(1)} %get-tuple-element.37), channel_id=1, source_target_pairs={{0,4},{1,5},{2,6},{3,7},{4,0},{5,1},{6,2},{7,3},{8,12},{9,13},{10,... | collective-permute-start | bytes 1572872 | tf_op jit(solution)/shard_map/ppermute | solution.py:30
  77.1 7.4 %expert.2 = (bf16[48,2048]{1,0:T(8,128)(2,1)S(1)}, bf16[48,2048]{1,0:T(8,128)(2,1)S(1)}, bf16[48,2048]{1,0:T(8,128)(2,1)S(1)}, bf16[48,2048]{1,0:T(8,128)(2,1)S(...) custom-call(bf16[48,2048]{1,0:T(8,128)(2,1)S(1)} %get-tuple-element.39.refs_0_, ...), custom_call_target="tpu_custom_call" | custom-call | flops 4227858432 | bytes 22020096 | tf_op jit(solution)/shard_map/expert/pallas_call | solution.py:354
  85.6 2.4 %collective-permute-start.17 = (bf16[48,2048]{1,0:T(8,128)(2,1)S(1)}, bf16[48,2048]{1,0:T(8,128)(2,1)S(1)}, u32[]{:S(2)}, u32[]{:S(2)}) collective-permute-start(bf16[48,2048]{1,0:T(8,128)(2,1)S(1)} %get-tuple-element.46), channel_id=1, source_target_pairs={{0,24},{8,16},{16,8},{24,0},{1,25},{9,17},{17,9},{25,1},{2,26},{10... | collective-permute-start | bytes 589832 | tf_op jit(solution)/shard_map/ppermute | solution.py:30
  88.1 5.3 %expert.3 = (bf16[48,2048]{1,0:T(8,128)(2,1)S(1)}, bf16[48,2048]{1,0:T(8,128)(2,1)S(1)}, bf16[48,2048]{1,0:T(8,128)(2,1)S(1)}, bf16[48,2048]{1,0:T(8,128)(2,1)S(1)}) custom-call(bf16[48,2048]{1,0:T(8,128)(2,1)S(1)} %get-tuple-element.49.refs_0_, bf16[48,2048]{1,0:T(8,128)(2,1)S(1)} %collective-permute-done.21.refs_1_, ...), custom_call_target="tpu_custom_call" | custom-call | flops 4227858432 | bytes 22020096 | tf_op jit(solution)/shard_map/expert/pallas_call | solution.py:354
  94.5 2.4 %collective-permute-start.26 = (bf16[48,2048]{1,0:T(8,128)(2,1)S(1)}, bf16[48,2048]{1,0:T(8,128)(2,1)S(1)}, u32[]{:S(2)}, u32[]{:S(2)}) collective-permute-start(bf16[48,2048]{1,0:T(8,128)(2,1)S(1)} %get-tuple-element.59), channel_id=1, source_target_pairs={{0,24},{8,16},{16,8},{24,0},{1,25},{9,17},{17,9},{25,1},{2,26},{10... | collective-permute-start | bytes 589832 | tf_op jit(solution)/shard_map/ppermute | solution.py:30
  98.4 1.8 %collective-permute-start.18 = (bf16[32,2048]{1,0:T(8,128)(2,1)S(1)}, bf16[32,2048]{1,0:T(8,128)(2,1)S(1)}, u32[]{:S(2)}, u32[]{:S(2)}) collective-permute-start(bf16[32,2048]{1,0:T(8,128)(2,1)S(1)} %get-tuple-element.48), channel_id=1, source_target_pairs={{0,2},{1,3},{2,0},{3,1},{4,6},{5,7},{6,4},{7,5},{8,10},{9,11},{10,... | collective-permute-start | bytes 393224 | tf_op jit(solution)/shard_map/ppermute | solution.py:30
  100.2 1.8 %collective-permute-done.25.refs_2_ = bf16[48,2048]{1,0:T(8,128)(2,1)S(1)} collective-permute-done((bf16[48,2048]{1,0:T(8,128)(2,1)S(1)}, bf16[48,2048]{1,0:T(8,128)(2,1)S(1)}, u32[]{:S(2)}, u32[]{:S(2)}) %collective-permute-start.25) | collective-permute-done | bytes 196640 | tf_op jit(solution)/shard_map/ppermute | solution.py:30
  103.1 3.8 %collective-permute-start.28 = (bf16[32,2048]{1,0:T(8,128)(2,1)S(1)}, bf16[32,2048]{1,0:T(8,128)(2,1)S(1)}, u32[]{:S(2)}, u32[]{:S(2)}) collective-permute-start(bf16[32,2048]{1,0:T(8,128)(2,1)S(1)} %get-tuple-element.61), channel_id=1, source_target_pairs={{0,6},{1,7},{2,4},{3,5},{4,2},{5,3},{6,0},{7,1},{8,14},{9,15},{10,... | collective-permute-start | bytes 393224 | tf_op jit(solution)/shard_map/ppermute | solution.py:30
  107.8 4.5 %collective-permute-done.27 = bf16[32,2048]{1,0:T(8,128)(2,1)S(1)} collective-permute-done((bf16[32,2048]{1,0:T(8,128)(2,1)S(1)}, bf16[32,2048]{1,0:T(8,128)(2,1)S(1)}, u32[]{:S(2)}, u32[]{:S(2)}) %collective-permute-start.27) | collective-permute-done | bytes 131104 | tf_op jit(solution)/shard_map/ppermute | solution.py:30
  (58 shorter events, 18.5 us)
Async XLA Ops:
  0.6 71.2 %collective-permute-start.12 = (bf16[2048,896]{1,0:T(8,128)(2,1)}, bf16[2048,896]{1,0:T(8,128)(2,1)}, u32[]{:S(2)}, u32[]{:S(2)}) collective-permute-start(bf16[2048,896]{1,0:T(8,128)(2,1)} %bitcast.9), channel_id=1, source_target_pairs={{0,1},{1,0},{2,3},{3,2},{4,5},{5,4},{6,7},{7,6},{8,9},{9,8},{10,11... | collective-permute-start | bytes 11010056 | tf_op jit(solution)/shard_map/ppermute | solution.py:30
  1.2 72.9 %collective-permute-start.13 = (bf16[2048,896]{1,0:T(8,128)(2,1)}, bf16[2048,896]{1,0:T(8,128)(2,1)}, u32[]{:S(2)}, u32[]{:S(2)}) collective-permute-start(bf16[2048,896]{1,0:T(8,128)(2,1)} %bitcast.12), channel_id=1, source_target_pairs={{0,1},{1,0},{2,3},{3,2},{4,5},{5,4},{6,7},{7,6},{8,9},{9,8},{10,11... | collective-permute-start | bytes 11010056 | tf_op jit(solution)/shard_map/ppermute | solution.py:30
  1.3 75.8 %collective-permute-start.14 = (bf16[896,2048]{1,0:T(8,128)(2,1)}, bf16[896,2048]{1,0:T(8,128)(2,1)}, u32[]{:S(2)}, u32[]{:S(2)}) collective-permute-start(bf16[896,2048]{1,0:T(8,128)(2,1)} %bitcast.15), channel_id=1, source_target_pairs={{0,1},{1,0},{2,3},{3,2},{4,5},{5,4},{6,7},{7,6},{8,9},{9,8},{10,11... | collective-permute-start | bytes 11010056 | tf_op jit(solution)/shard_map/ppermute | solution.py:30
  2.9 19.1 %collective-permute-start.8 = (bf16[32,2176]{1,0:T(8,128)(2,1)S(1)}, bf16[32,2176]{1,0:T(8,128)(2,1)S(1)}, u32[]{:S(2)}, u32[]{:S(2)}) collective-permute-start(bf16[32,2176]{1,0:T(8,128)(2,1)S(1)} %get-tuple-element.38.refs_0_), channel_id=1, source_target_pairs={{0,2},{1,3},{2,0},{3,1},{4,6},{5,7},{6,4},{7,5},{8,10},{9,11},{10,... | collective-permute-start | bytes 417800 | tf_op jit(solution)/shard_map/ppermute | solution.py:30
  18.1 14.4 %collective-permute-start.19 = (bf16[32,2176]{1,0:T(8,128)(2,1)S(1)}, bf16[32,2176]{1,0:T(8,128)(2,1)S(1)}, u32[]{:S(2)}, u32[]{:S(2)}) collective-permute-start(bf16[32,2176]{1,0:T(8,128)(2,1)S(1)} %get-tuple-element.38.refs_0_), channel_id=1, source_target_pairs={{0,4},{1,5},{2,6},{3,7},{4,0},{5,1},{6,2},{7,3},{8,12},{9,13},{10,... | collective-permute-start | bytes 417800 | tf_op jit(solution)/shard_map/ppermute | solution.py:30
  22.0 10.7 %collective-permute-start.20 = (bf16[32,2176]{1,0:T(8,128)(2,1)S(1)}, bf16[32,2176]{1,0:T(8,128)(2,1)S(1)}, u32[]{:S(2)}, u32[]{:S(2)}) collective-permute-start(bf16[32,2176]{1,0:T(8,128)(2,1)S(1)} %get-tuple-element.38.refs_0_), channel_id=1, source_target_pairs={{0,6},{1,7},{2,4},{3,5},{4,2},{5,3},{6,0},{7,1},{8,14},{9,15},{10,... | collective-permute-start | bytes 417800 | tf_op jit(solution)/shard_map/ppermute | solution.py:30
  32.5 24.0 %collective-permute-start.5 = (bf16[128,2048]{1,0:T(8,128)(2,1)S(1)}, bf16[128,2048]{1,0:T(8,128)(2,1)S(1)}, u32[]{:S(2)}, u32[]{:S(2)}) collective-permute-start(bf16[128,2048]{1,0:T(8,128)(2,1)S(1)} %copy-done.3), channel_id=1, source_target_pairs={{0,2},{1,3},{2,0},{3,1},{4,6},{5,7},{6,4},{7,5},{8,10},{9,11},{10,... | collective-permute-start | bytes 1572872 | tf_op jit(solution)/shard_map/ppermute | solution.py:30
  32.8 15.4 %collective-permute-start.2 = (bf16[512,128]{1,0:T(8,128)(2,1)S(1)}, bf16[512,128]{1,0:T(8,128)(2,1)S(1)}, u32[]{:S(2)}, u32[]{:S(2)}) collective-permute-start(bf16[512,128]{1,0:T(8,128)(2,1)S(1)} %get-tuple-element.35), channel_id=1, source_target_pairs={{0,2},{1,3},{2,0},{3,1},{4,6},{5,7},{6,4},{7,5},{8,10},{9,11},{10,... | collective-permute-start | bytes 393224 | tf_op jit(solution)/shard_map/ppermute | solution.py:30
  49.5 7.0 %collective-permute-start.10 = (bf16[48,2048]{1,0:T(8,128)(2,1)S(1)}, bf16[48,2048]{1,0:T(8,128)(2,1)S(1)}, u32[]{:S(2)}, u32[]{:S(2)}) collective-permute-start(bf16[48,2048]{1,0:T(8,128)(2,1)S(1)} %get-tuple-element.41), channel_id=1, source_target_pairs={{0,16},{8,24},{16,0},{24,8},{1,17},{9,25},{17,1},{25,9},{2,18},{10... | collective-permute-start | bytes 589832 | tf_op jit(solution)/shard_map/ppermute | solution.py:30
  58.4 8.7 %collective-permute-start.11 = (bf16[48,2048]{1,0:T(8,128)(2,1)S(1)}, bf16[48,2048]{1,0:T(8,128)(2,1)S(1)}, u32[]{:S(2)}, u32[]{:S(2)}) collective-permute-start(bf16[48,2048]{1,0:T(8,128)(2,1)S(1)} %get-tuple-element.42), channel_id=1, source_target_pairs={{0,24},{8,16},{16,8},{24,0},{1,25},{9,17},{17,9},{25,1},{2,26},{10... | collective-permute-start | bytes 589832 | tf_op jit(solution)/shard_map/ppermute | solution.py:30
  60.6 10.5 %collective-permute-start.9 = (bf16[48,2048]{1,0:T(8,128)(2,1)S(1)}, bf16[48,2048]{1,0:T(8,128)(2,1)S(1)}, u32[]{:S(2)}, u32[]{:S(2)}) collective-permute-start(bf16[48,2048]{1,0:T(8,128)(2,1)S(1)} %get-tuple-element.40), channel_id=1, source_target_pairs={{0,8},{8,0},{16,24},{24,16},{1,9},{9,1},{17,25},{25,17},{2,10},{10... | collective-permute-start | bytes 589832 | tf_op jit(solution)/shard_map/ppermute | solution.py:30
  67.0 18.1 %collective-permute-start.21 = (bf16[48,2048]{1,0:T(8,128)(2,1)S(1)}, bf16[48,2048]{1,0:T(8,128)(2,1)S(1)}, u32[]{:S(2)}, u32[]{:S(2)}) collective-permute-start(bf16[48,2048]{1,0:T(8,128)(2,1)S(1)} %get-tuple-element.50), channel_id=1, source_target_pairs={{0,8},{8,0},{16,24},{24,16},{1,9},{9,1},{17,25},{25,17},{2,10},{10... | collective-permute-start | bytes 589832 | tf_op jit(solution)/shard_map/ppermute | solution.py:30
  71.1 14.6 %collective-permute-start.22 = (bf16[48,2048]{1,0:T(8,128)(2,1)S(1)}, bf16[48,2048]{1,0:T(8,128)(2,1)S(1)}, u32[]{:S(2)}, u32[]{:S(2)}) collective-permute-start(bf16[48,2048]{1,0:T(8,128)(2,1)S(1)} %get-tuple-element.51), channel_id=1, source_target_pairs={{0,16},{8,24},{16,0},{24,8},{1,17},{9,25},{17,1},{25,9},{2,18},{10... | collective-permute-start | bytes 589832 | tf_op jit(solution)/shard_map/ppermute | solution.py:30
  71.8 16.3 %collective-permute-start.23 = (bf16[48,2048]{1,0:T(8,128)(2,1)S(1)}, bf16[48,2048]{1,0:T(8,128)(2,1)S(1)}, u32[]{:S(2)}, u32[]{:S(2)}) collective-permute-start(bf16[48,2048]{1,0:T(8,128)(2,1)S(1)} %get-tuple-element.52), channel_id=1, source_target_pairs={{0,24},{8,16},{16,8},{24,0},{1,25},{9,17},{17,9},{25,1},{2,26},{10... | collective-permute-start | bytes 589832 | tf_op jit(solution)/shard_map/ppermute | solution.py:30
  74.0 32.9 %collective-permute-start.7 = (bf16[128,2048]{1,0:T(8,128)(2,1)S(1)}, bf16[128,2048]{1,0:T(8,128)(2,1)S(1)}, u32[]{:S(2)}, u32[]{:S(2)}) collective-permute-start(bf16[128,2048]{1,0:T(8,128)(2,1)S(1)} %get-tuple-element.37), channel_id=1, source_target_pairs={{0,4},{1,5},{2,6},{3,7},{4,0},{5,1},{6,2},{7,3},{8,12},{9,13},{10,... | collective-permute-start | bytes 1572872 | tf_op jit(solution)/shard_map/ppermute | solution.py:30
  84.5 9.4 %collective-permute-start.15 = (bf16[48,2048]{1,0:T(8,128)(2,1)S(1)}, bf16[48,2048]{1,0:T(8,128)(2,1)S(1)}, u32[]{:S(2)}, u32[]{:S(2)}) collective-permute-start(bf16[48,2048]{1,0:T(8,128)(2,1)S(1)} %get-tuple-element.44), channel_id=1, source_target_pairs={{0,8},{8,0},{16,24},{24,16},{1,9},{9,1},{17,25},{25,17},{2,10},{10... | collective-permute-start | bytes 589832 | tf_op jit(solution)/shard_map/ppermute | solution.py:30
  85.1 9.3 %collective-permute-start.16 = (bf16[48,2048]{1,0:T(8,128)(2,1)S(1)}, bf16[48,2048]{1,0:T(8,128)(2,1)S(1)}, u32[]{:S(2)}, u32[]{:S(2)}) collective-permute-start(bf16[48,2048]{1,0:T(8,128)(2,1)S(1)} %get-tuple-element.45), channel_id=1, source_target_pairs={{0,16},{8,24},{16,0},{24,8},{1,17},{9,25},{17,1},{25,9},{2,18},{10... | collective-permute-start | bytes 589832 | tf_op jit(solution)/shard_map/ppermute | solution.py:30
  85.6 12.0 %collective-permute-start.17 = (bf16[48,2048]{1,0:T(8,128)(2,1)S(1)}, bf16[48,2048]{1,0:T(8,128)(2,1)S(1)}, u32[]{:S(2)}, u32[]{:S(2)}) collective-permute-start(bf16[48,2048]{1,0:T(8,128)(2,1)S(1)} %get-tuple-element.46), channel_id=1, source_target_pairs={{0,24},{8,16},{16,8},{24,0},{1,25},{9,17},{17,9},{25,1},{2,26},{10... | collective-permute-start | bytes 589832 | tf_op jit(solution)/shard_map/ppermute | solution.py:30
  93.4 6.8 %collective-permute-start.24 = (bf16[48,2048]{1,0:T(8,128)(2,1)S(1)}, bf16[48,2048]{1,0:T(8,128)(2,1)S(1)}, u32[]{:S(2)}, u32[]{:S(2)}) collective-permute-start(bf16[48,2048]{1,0:T(8,128)(2,1)S(1)} %get-tuple-element.57), channel_id=1, source_target_pairs={{0,8},{8,0},{16,24},{24,16},{1,9},{9,1},{17,25},{25,17},{2,10},{10... | collective-permute-start | bytes 589832 | tf_op jit(solution)/shard_map/ppermute | solution.py:30
  94.0 8.1 %collective-permute-start.25 = (bf16[48,2048]{1,0:T(8,128)(2,1)S(1)}, bf16[48,2048]{1,0:T(8,128)(2,1)S(1)}, u32[]{:S(2)}, u32[]{:S(2)}) collective-permute-start(bf16[48,2048]{1,0:T(8,128)(2,1)S(1)} %get-tuple-element.58), channel_id=1, source_target_pairs={{0,16},{8,24},{16,0},{24,8},{1,17},{9,25},{17,1},{25,9},{2,18},{10... | collective-permute-start | bytes 589832 | tf_op jit(solution)/shard_map/ppermute | solution.py:30
  94.5 7.5 %collective-permute-start.26 = (bf16[48,2048]{1,0:T(8,128)(2,1)S(1)}, bf16[48,2048]{1,0:T(8,128)(2,1)S(1)}, u32[]{:S(2)}, u32[]{:S(2)}) collective-permute-start(bf16[48,2048]{1,0:T(8,128)(2,1)S(1)} %get-tuple-element.59), channel_id=1, source_target_pairs={{0,24},{8,16},{16,8},{24,0},{1,25},{9,17},{17,9},{25,1},{2,26},{10... | collective-permute-start | bytes 589832 | tf_op jit(solution)/shard_map/ppermute | solution.py:30
  98.4 9.4 %collective-permute-start.18 = (bf16[32,2048]{1,0:T(8,128)(2,1)S(1)}, bf16[32,2048]{1,0:T(8,128)(2,1)S(1)}, u32[]{:S(2)}, u32[]{:S(2)}) collective-permute-start(bf16[32,2048]{1,0:T(8,128)(2,1)S(1)} %get-tuple-element.48), channel_id=1, source_target_pairs={{0,2},{1,3},{2,0},{3,1},{4,6},{5,7},{6,4},{7,5},{8,10},{9,11},{10,... | collective-permute-start | bytes 393224 | tf_op jit(solution)/shard_map/ppermute | solution.py:30
  102.7 9.6 %collective-permute-start.27 = (bf16[32,2048]{1,0:T(8,128)(2,1)S(1)}, bf16[32,2048]{1,0:T(8,128)(2,1)S(1)}, u32[]{:S(2)}, u32[]{:S(2)}) collective-permute-start(bf16[32,2048]{1,0:T(8,128)(2,1)S(1)} %get-tuple-element.60), channel_id=1, source_target_pairs={{0,4},{1,5},{2,6},{3,7},{4,0},{5,1},{6,2},{7,3},{8,12},{9,13},{10,... | collective-permute-start | bytes 393224 | tf_op jit(solution)/shard_map/ppermute | solution.py:30
  103.1 9.2 %collective-permute-start.28 = (bf16[32,2048]{1,0:T(8,128)(2,1)S(1)}, bf16[32,2048]{1,0:T(8,128)(2,1)S(1)}, u32[]{:S(2)}, u32[]{:S(2)}) collective-permute-start(bf16[32,2048]{1,0:T(8,128)(2,1)S(1)} %get-tuple-element.61), channel_id=1, source_target_pairs={{0,6},{1,7},{2,4},{3,5},{4,2},{5,3},{6,0},{7,1},{8,14},{9,15},{10,... | collective-permute-start | bytes 393224 | tf_op jit(solution)/shard_map/ppermute | solution.py:30
  (10 other events, 136.1 us)
